TPU v7x, 32 devices: a whole 2x2x4 slice. The times are simulated.
32 devices in a mesh: grp: 2 (over x), ep: 16 (over z, y, core).
Axes of the slice: x: 2, y: 2, z: 4, core: 2. Of those that a mesh axis runs over, the one named last changes fastest.
Arguments:
- tokens: bfloat16 [128, 2048], P(('grp', 'ep')), parts along dimension 0, may hold values from -6 to 6
- lengths: int32 [128], P(('grp', 'ep')), parts along dimension 0, may hold values from 128 to 1024, as said below
- cache_key: bfloat16 [128, 1024, 256], P(('grp', 'ep')), parts along dimension 0, may hold values from -6 to 6
- cache_value: bfloat16 [128, 1024, 256], P(('grp', 'ep')), parts along dimension 0, may hold values from -6 to 6
- routes: int32 [128, 2], P(('grp', 'ep')), parts along dimension 0, may hold values from 0 to 3, all different within a row
- route_logits: float32 [128, 2], P(('grp', 'ep')), parts along dimension 0, may hold values from -6 to 6
- mix_gain: float32 [2048], replicated, may hold values from 0.1 to 1.9
- query_gain: float32 [64], replicated, may hold values from 0.1 to 1.9
- key_gain: float32 [64], replicated, may hold values from 0.1 to 1.9
- head_bias: float32 [16], replicated, may hold values from -9 to -3.5
- w_query: bfloat16 [2048, 1024], P('ep'), may hold values from -0.125 to 0.125
- w_key: bfloat16 [2048, 256], P('ep'), may hold values from -0.125 to 0.125
- w_value: bfloat16 [2048, 256], P('ep'), may hold values from -0.125 to 0.125
- w_out: bfloat16 [1024, 2048], P(None, 'ep'), may hold values from -0.1875 to 0.1875
- ffn_gain: float32 [2048], replicated, may hold values from 0.1 to 1.9
- w_gate: bfloat16 [2048, 28672], P(None, 'ep'), may hold values from -0.125 to 0.125
- w_up: bfloat16 [2048, 28672], P(None, 'ep'), may hold values from -0.125 to 0.125
- w_down: bfloat16 [28672, 2048], P('ep'), may hold values from -0.0625 to 0.0625
Outputs:
- output: bfloat16 [128, 2048], P(('grp', 'ep')), parts along dimension 0
- new_key: bfloat16 [128, 256], P(('grp', 'ep')), parts along dimension 0
- new_value: bfloat16 [128, 256], P(('grp', 'ep')), parts along dimension 0
There are 2 independent parts, one for each index of `grp`. A program takes and returns all parts, laid end to end along the dimension named above; an argument that names none is the same for every part. Nothing has to cross between parts.
Inputs may be any that keep to these rules, and one draw needn't show every extreme that they name: `lengths`: some sequence has all 1024 positions live.
All inputs are finite; a program needn't handle non-finite values.
Results may differ from a plain program's by a relative error of at most 0.0085.
Values may be sent and summed in bfloat16 or wider, within the bound.
No kernel may reach another device: no remote copies, remote signals or barrier semaphores. Data moves between devices by JAX's collectives and lax.ppermute only.
A program may use at most 128 MiB of HBM per device.

v0:
```python
import jax
import jax.numpy as jnp
from jax import lax
from jax.sharding import PartitionSpec as P

HEADS = 16
KV_HEADS = 4
HEAD_DIM = 64
FF = 7168
EXPERTS = 4


EPSILON = 1e-06


def rms_scaled(values, gain):
    return values * lax.rsqrt(jnp.mean(values * values, axis=-1, keepdims=True) + EPSILON) * gain


def route_weights(routes, route_logits):
    experts_iota = jnp.arange(EXPERTS, dtype=jnp.int32)[None, :]
    first_share = jax.nn.sigmoid(route_logits[:, 0:1] - route_logits[:, 1:2])
    second_share = jax.nn.sigmoid(route_logits[:, 1:2] - route_logits[:, 0:1])
    return jnp.where(routes[:, 0:1] == experts_iota, first_share, 0.0) + jnp.where(
        routes[:, 1:2] == experts_iota, second_share, 0.0
    )


def stick_attend(queries, lengths, cache_key, cache_value, query_gain, head_bias):
    batch_rows = queries.shape[0]
    cache_len = cache_key.shape[1]
    group_size = HEADS // KV_HEADS
    normed_query = rms_scaled(queries.reshape(batch_rows, HEADS, HEAD_DIM), query_gain).astype(
        jnp.bfloat16
    )
    normed_query = normed_query.reshape(batch_rows, KV_HEADS, group_size, HEAD_DIM)
    key_heads = cache_key.reshape(batch_rows, cache_len, KV_HEADS, HEAD_DIM)
    value_heads = cache_value.reshape(batch_rows, cache_len, KV_HEADS, HEAD_DIM)
    scores = jnp.einsum(
        "bkgd,blkd->bkgl", normed_query, key_heads, preferred_element_type=jnp.float32
    ) * HEAD_DIM ** (-0.5)
    scores = scores + head_bias.reshape(KV_HEADS, group_size)[None, :, :, None]
    live_mask = (
        jnp.arange(cache_len, dtype=jnp.int32)[None, None, None, :] < lengths[:, None, None, None]
    )
    remain = jnp.where(live_mask, jax.nn.log_sigmoid(-scores), 0.0)
    after_sum = lax.cumsum(remain, axis=3, reverse=True) - remain
    weights = jnp.where(live_mask, jnp.exp(jax.nn.log_sigmoid(scores) + after_sum), 0.0).astype(
        jnp.bfloat16
    )
    attended = jnp.einsum(
        "bkgl,blkd->bkgd", weights, value_heads, preferred_element_type=jnp.float32
    )
    return attended.reshape(batch_rows, HEADS * HEAD_DIM).astype(jnp.bfloat16)


def local(
    tokens,
    lengths,
    cache_key,
    cache_value,
    routes,
    route_logits,
    mix_gain,
    query_gain,
    key_gain,
    head_bias,
    w_query,
    w_key,
    w_value,
    w_out,
    ffn_gain,
    w_gate,
    w_up,
    w_down,
):
    token_rows = tokens.shape[0]
    key_width = w_key.shape[1]
    as_float = tokens.astype(jnp.float32)
    normed = rms_scaled(as_float, mix_gain).astype(jnp.bfloat16)
    pieces = (
        lax.all_gather(w_query, "ep", axis=0, tiled=True),
        lax.all_gather(w_key, "ep", axis=0, tiled=True),
        lax.all_gather(w_value, "ep", axis=0, tiled=True),
    )
    queries, fresh_key, fresh_value = tuple(
        (jnp.dot(normed, weight, preferred_element_type=jnp.float32) for weight in pieces)
    )
    new_key = rms_scaled(fresh_key.reshape(token_rows, KV_HEADS, HEAD_DIM), key_gain)
    new_key = new_key.reshape(token_rows, key_width).astype(jnp.bfloat16)
    new_value = fresh_value.astype(jnp.bfloat16)
    attended = stick_attend(queries, lengths, cache_key, cache_value, query_gain, head_bias)
    mixed = as_float + jnp.dot(
        attended,
        lax.all_gather(w_out, "ep", axis=1, tiled=True),
        preferred_element_type=jnp.float32,
    )
    expert_in = rms_scaled(mixed, ffn_gain).astype(jnp.bfloat16)
    every_gate = lax.all_gather(route_weights(routes, route_logits), "ep", axis=0, tiled=True)
    ff_share = w_gate.shape[1]
    my_expert = lax.axis_index("ep") // (FF // ff_share)
    my_gate = lax.dynamic_slice_in_dim(every_gate, my_expert, 1, 1)
    input_rows = lax.all_gather(expert_in, "ep", axis=0, tiled=True)
    gate_value = jnp.dot(input_rows, w_gate, preferred_element_type=jnp.float32)
    up_value = jnp.dot(input_rows, w_up, preferred_element_type=jnp.float32)
    hidden = (jax.nn.silu(gate_value) * up_value * my_gate).astype(jnp.bfloat16)
    expert_sum = lax.psum_scatter(
        jnp.dot(hidden, w_down, preferred_element_type=jnp.float32),
        "ep",
        scatter_dimension=0,
        tiled=True,
    )
    return ((mixed + expert_sum).astype(jnp.bfloat16), new_key, new_value)


def solution(mesh):
    return jax.shard_map(
        local,
        mesh=mesh,
        in_specs=(
            P(("grp", "ep"), None),
            P(("grp", "ep")),
            P(("grp", "ep"), None, None),
            P(("grp", "ep"), None, None),
            P(("grp", "ep"), None),
            P(("grp", "ep"), None),
            P(),
            P(),
            P(),
            P(),
            P("ep", None),
            P("ep", None),
            P("ep", None),
            P(None, "ep"),
            P(),
            P(None, "ep"),
            P(None, "ep"),
            P("ep", None),
        ),
        out_specs=(P(("grp", "ep"), None), P(("grp", "ep"), None), P(("grp", "ep"), None)),
        check_vma=False,
    )
```

profile of v0, /device:TPU:0, one launch (start us, length us, event | category | flops | bytes accessed | tf_op | source)
XLA Modules:
  0.0 323.6 jit_solution(14233699592130676212)
XLA Ops:
  7.2 0.7 all-gather.11.cloned.1.call-update
  8.0 0.7 all-gather.7.cloned.1.call-update
  8.7 0.7 all-gather.9.cloned.1.call-update
  9.4 0.5 all-gather.13.cloned.1.call-update
  10.1 0.8 slice_bitcast_fusion.1
  10.8 0.8 divide_bitcast_fusion.1
  11.6 23.2 %all-gather.1 = f32[16,4,4]{2,1,0:T(4,128)S(1)} all-gather(f32[1,4,4]{2,1,0:T(4,128)S(1)} %add_bitcast_fusion), channel_id=1, replica_groups=mesh['grp'=2,'ep'=16] {'ep'}, dimensions={0}, use_global_device_ids=true | all-gather | bytes 1088 | tf_op jit(solution)/shard_map/all_gather | solution.py:99
  35.0 0.9 fusion.21
  35.9 0.7 iota_compare_fusion
  36.6 4.0 %copy.27 = bf16[4,1024,256]{1,2,0:T(8,128)(2,1)} copy(bf16[4,1024,256]{2,1,0:T(8,128)(2,1)} %param.20) | data formatting | bytes 4194304 | tf_op args[2]
  40.7 2.6 copy.28
  43.3 0.6 dynamic-slice
  44.6 6.3 %all-gather.11.cloned.1.call-done = bf16[2048,256]{1,0:T(8,128)(2,1)} async-done(((bf16[128,256]{1,0:T(8,128)(2,1)}), bf16[2048,256]{1,0:T(8,128)(2,1)}) %all-gather.11.cloned.1.call-update) | async-done | bytes 1048592 | tf_op jit(solution)/shard_map/all_gather | solution.py:83
  50.8 1.5 fusion.37
  52.7 49.7 %all-gather.7.cloned.1.call-done = bf16[2048,1024]{1,0:T(8,128)(2,1)} async-done(((bf16[128,1024]{1,0:T(8,128)(2,1)}), bf16[2048,1024]{1,0:T(8,128)(2,1)}) %all-gather.7.cloned.1.call-update) | async-done | bytes 4194320 | tf_op jit(solution)/shard_map/all_gather | solution.py:82
  102.4 2.9 fusion.36
  105.5 0.1 reshape.101
  105.6 2.2 fusion.15
  107.9 0.1 reshape.103
  108.0 79.2 %reduce-window.6 = f32[4,4,4,8,128]{4,3,2,1,0:T(8,128)S(1)} reduce-window(f32[4,4,4,8,128]{4,3,2,1,0:T(8,128)S(1)} %reshape.103, f32[]{:T(128)} %constant.36.clone.1), window={size=1x1x1x1x128 pad=0_0x0_0x0_0x0_0x0_127}, to_apply=%region_2.0 | reduce-window | flops 8323072 | bytes 524292 | tf_op jit(solution)/shard_map/reduce-window
  187.2 0.2 slice_reduce_fusion
  187.4 2.8 reduce-window.9
  190.3 0.1 broadcast_add_fusion
  190.6 0.9 convolution_convert_fusion
  191.6 3.0 multiply_reduce_fusion
  194.7 19.6 %all-gather = bf16[16,4,2048]{2,1,0:T(4,128)(2,1)S(1)} all-gather(bf16[1,4,2048]{2,1,0:T(4,128)(2,1)S(1)} %fusion.25), channel_id=1, replica_groups=mesh['grp'=2,'ep'=16] {'ep'}, dimensions={0}, use_global_device_ids=true | all-gather | bytes 278528 | tf_op jit(solution)/shard_map/all_gather | solution.py:103
  214.4 4.4 %fusion.38 = f32[64,1792]{1,0:T(8,128)S(1)} fusion(bf16[64,2048]{1,0:T(8,128)(2,1)S(1)} %reshape.107, bf16[2048,1792]{1,0:T(8,128)(2,1)} %param.33), kind=kOutput, calls=%fused_computation.62 | convolution fusion | flops 469762048 | bytes 8060928 | tf_op jit(solution)/shard_map/dot_general | solution.py:104
  218.8 8.7 %fusion.3 = f32[64,2048]{1,0:T(8,128)} fusion(bf16[1792,2048]{1,0:T(8,128)(2,1)} %param.35, bf16[64,2048]{1,0:T(8,128)(2,1)S(1)} %reshape.107, bf16[2048,1792]{1,0:T(8,128)(2,1)} %param.34, f32[64,1792]{1,0:T(8,128)S(1)} %fusion.38, f32[64]{0:T(128)S(1)} %bitcast.34), kind=kOutput, calls=%fused_computation.8 | convolution fusion | flops 940326912 | bytes 15925504 | tf_op jit(solution)/shard_map/dot_general | solution.py:108
  227.5 0.6 multiply_convert_fusion.3
  228.1 2.1 convolution_convert_fusion.1
  230.2 85.5 %all-reduce.3.cloned.1.call-done = f32[64,2048]{1,0:T(8,128)} async-done(((f32[64,2048]{1,0:T(8,128)}), f32[64,2048]{1,0:T(8,128)}) %all-reduce.3.cloned.1.call-update) | async-done | bytes 524304
  315.7 1.5 fusion.24
  (48 shorter events, 1.7 us)
Async XLA Ops:
  7.2 33.4 %copy-start.5 = (f32[16]{0:T(128)S(1)}, f32[16]{0:T(128)}, u32[]{:S(2)}) copy-start(f32[16]{0:T(128)} %param.27) | copy-start | bytes 196
  7.2 33.5 %copy-start = (bf16[4,1024,256]{2,1,0:T(8,128)(2,1)S(1)}, bf16[4,1024,256]{2,1,0:T(8,128)(2,1)}, u32[]{:S(2)}) copy-start(bf16[4,1024,256]{2,1,0:T(8,128)(2,1)} %param.21) | copy-start | bytes 6291460
  7.2 43.6 %all-gather.11.cloned.1.call-start = ((), (), s32[]{:S(2)}) async-start(), calls=%async_computation.2 | async-start | bytes 1114112 | tf_op jit(solution)/shard_map/all_gather | solution.py:83
  7.9 94.5 %all-gather.7.cloned.1.call-start = ((), (), s32[]{:S(2)}) async-start(), calls=%async_computation | async-start | bytes 4456448 | tf_op jit(solution)/shard_map/all_gather | solution.py:82
  8.7 182.9 %all-gather.9.cloned.1.call-start = ((), (), s32[]{:S(2)}) async-start(), calls=%async_computation.1 | async-start | bytes 4456448 | tf_op jit(solution)/shard_map/all_gather | solution.py:95
  9.4 218.7 %all-gather.13.cloned.1.call-start = ((), (), s32[]{:S(2)}) async-start(), calls=%async_computation.3 | async-start | bytes 1114112 | tf_op jit(solution)/shard_map/all_gather | solution.py:84
  10.0 305.7 %all-reduce.3.cloned.1.call-start = ((), (), s32[]{:S(2)}) async-start(), calls=%async_computation.4 | async-start | bytes 1048576
  36.6 6.7 %copy-start.6 = (f32[64]{0:T(128)S(1)}, f32[64]{0:T(128)}, u32[]{:S(2)}) copy-start(f32[64]{0:T(128)} %param.26) | copy-start | bytes 772
  36.6 6.7 %copy-start.8 = (u32[32]{0:T(128)S(1)}, u32[32]{0:T(128)}, u32[]{:S(2)}) copy-start(u32[32]{0:T(128)} %constant.57) | copy-start | bytes 388
  36.6 14.2 %copy-start.2 = (bf16[4,2048]{1,0:T(4,128)(2,1)S(1)}, bf16[4,2048]{1,0:T(4,128)(2,1)}, u32[]{:S(2)}) copy-start(bf16[4,2048]{1,0:T(4,128)(2,1)} %param.18) | copy-start | bytes 49156
  36.6 14.2 %copy-start.3 = (f32[2048]{0:T(1024)S(1)}, f32[2048]{0:T(1024)}, u32[]{:S(2)}) copy-start(f32[2048]{0:T(1024)} %param.24) | copy-start | bytes 24580
  40.7 64.9 %copy-start.7 = (f32[64]{0:T(128)S(1)}, f32[64]{0:T(128)}, u32[]{:S(2)}) copy-start(f32[64]{0:T(128)} %param.25) | copy-start | bytes 772
  52.7 137.9 %copy-start.1 = (bf16[4,1024,256]{1,2,0:T(8,128)(2,1)S(1)}, bf16[4,1024,256]{1,2,0:T(8,128)(2,1)}, u32[]{:S(2)}) copy-start(bf16[4,1024,256]{1,2,0:T(8,128)(2,1)} %copy.28) | copy-start | bytes 6291460
  190.6 4.1 %copy-start.4 = (f32[2048]{0:T(1024)S(1)}, f32[2048]{0:T(1024)}, u32[]{:S(2)}) copy-start(f32[2048]{0:T(1024)} %param.32) | copy-start | bytes 24580
Sparse Core Ops, SparseCore 0:
  10.2 40.6 all-gather.10
  53.0 49.3 all-gather.6
  104.5 50.9 all-gather.8
  157.6 36.2 all-gather.12
  227.7 87.9 all-reduce.2
where the time goes:
time: 324 us
  waiting for transfers between devices  144 us (44%)
  other arithmetic  87 us (27%)
  blocking collectives  42.8 us (13%)
  matrix products  25.7 us (8%)
  between operations  14.6 us (5%)
  local copies, waits for them, and re-layouts  9.35 us (3%)
    unnamed x6, waiting for transfers between devices  88 us
    another operation x2, other arithmetic  82.1 us
    all_gather x1, waiting for transfers between devices, local(): lax.all_gather(w_query, 'ep', axis=0, tiled=True)  49.7 us
    all_gather x1, blocking collectives, local(): lax.all_gather(route_weights(routes, route_logits), 'ep', axis=0, tiled=T...  23.2 us
    all_gather x1, blocking collectives, local(): input_rows = lax.all_gather(expert_in, 'ep', axis=0, tiled=True)  19.6 us
    dot_general x1, matrix products, local(): jnp.dot(hidden, w_down, preferred_element_type=jnp.float32)  8.67 us
    unnamed x23, local copies, waits for them, and re-layouts  7.29 us
  transfers between devices with their start and end apart: 5, of which 3 were waited for; matrix products, arithmetic and copies ran while one was open for 37% of the time, Pallas kernels for 0%

commit v1 on v0

v1 whole, which is shorter than its diff:
```python
import functools

import jax
import jax.numpy as jnp
from jax import lax
from jax.experimental import pallas as pl
from jax.experimental.pallas import tpu as pltpu
from jax.sharding import PartitionSpec as P

HEADS = 16
KV_HEADS = 4
HEAD_DIM = 64
FF = 7168
EXPERTS = 4
EPSILON = 1e-06

GROUP = HEADS // KV_HEADS
KEY_WIDTH = KV_HEADS * HEAD_DIM
QUERY_WIDTH = HEADS * HEAD_DIM
ROW_WIDTH = QUERY_WIDTH + 128
BLOCK = 256
F32 = jnp.float32
BF16 = jnp.bfloat16
VMEM = pltpu.VMEM
NT = (((1,), (1,)), ((), ()))


def vmem_spec():
    return pl.BlockSpec(memory_space=VMEM)


def smem_spec():
    return pl.BlockSpec(memory_space=pltpu.SMEM)


def project_kernel(rows_ref, gain_ref, wq_ref, wk_ref, wv_ref, out_ref):
    shards, tokens, width = rows_ref.shape
    rows = rows_ref[...].astype(F32).reshape(shards * tokens, width)
    scaled = (rows * gain_ref[...]).astype(BF16)
    start = 0
    for w_ref in (wq_ref, wk_ref, wv_ref):
        size = w_ref.shape[1]
        part = jnp.dot(scaled, w_ref[...], preferred_element_type=F32)
        out_ref[:, :, start : start + size] = part.astype(BF16).reshape(shards, tokens, size)
        start += size


def attend_kernel(
    lengths_ref,
    routes_ref,
    logits_ref,
    bias_ref,
    parts_ref,
    tokens_ref,
    qgain_ref,
    kgain_ref,
    key_ref,
    value_ref,
    row_ref,
    new_key_ref,
    new_value_ref,
    heads_scr,
):
    shards, tokens, _ = parts_ref.shape
    cache_len = key_ref.shape[1]
    columns = tokens * HEADS

    own = tokens_ref[...].astype(F32)
    token_scale = lax.rsqrt(jnp.mean(own * own, axis=-1, keepdims=True) + EPSILON)
    total = parts_ref[0].astype(F32)
    for shard in range(1, shards):
        total = total + parts_ref[shard].astype(F32)
    total = total * token_scale
    fresh_key = total[:, QUERY_WIDTH : QUERY_WIDTH + KEY_WIDTH]
    new_value_ref[...] = total[:, QUERY_WIDTH + KEY_WIDTH :].astype(BF16)

    lane = lax.broadcasted_iota(jnp.int32, (tokens, KEY_WIDTH), 1)
    squares = fresh_key * fresh_key
    key_scale = jnp.zeros_like(fresh_key)
    for head in range(KV_HEADS):
        mine = lane // HEAD_DIM == head
        mean = jnp.sum(jnp.where(mine, squares, 0.0), axis=-1, keepdims=True) / HEAD_DIM
        key_scale = jnp.where(mine, lax.rsqrt(mean + EPSILON), key_scale)
    new_key_ref[...] = (fresh_key * key_scale * kgain_ref[...]).astype(BF16)

    for member in range(GROUP):
        pieces = []
        for group in range(KV_HEADS):
            head = group * GROUP + member
            pieces.append(total[:, head * HEAD_DIM : (head + 1) * HEAD_DIM])
        heads_scr[:, member, :] = jnp.concatenate(pieces, axis=-1)
    stacked = []
    for token in range(tokens):
        stacked += [heads_scr[token]] * KV_HEADS
    query = jnp.concatenate(stacked, axis=0)
    row = lax.broadcasted_iota(jnp.int32, query.shape, 0)
    col = lax.broadcasted_iota(jnp.int32, query.shape, 1)
    query = jnp.where(row % HEADS // GROUP == col // HEAD_DIM, query, 0.0)
    query_mean = jnp.sum(query * query, axis=-1, keepdims=True) / HEAD_DIM
    query = query * lax.rsqrt(query_mean + EPSILON) * qgain_ref[...]
    query = query.astype(BF16).astype(F32)
    padded = [
        jnp.where(row // HEADS == token, query, 0.0).astype(BF16) for token in range(tokens)
    ]

    out_col = lax.broadcasted_iota(jnp.int32, (1, columns), 1)
    live = jnp.zeros((1, columns), jnp.int32)
    bias = jnp.zeros((1, columns), F32)
    for token in range(tokens):
        live = jnp.where(out_col // HEADS == token, lengths_ref[token], live)
    for head in range(HEADS):
        bias = jnp.where(out_col % HEADS == head, bias_ref[head], bias)

    upper = (
        lax.broadcasted_iota(jnp.int32, (BLOCK, BLOCK), 1)
        >= lax.broadcasted_iota(jnp.int32, (BLOCK, BLOCK), 0)
    ).astype(F32).astype(BF16)
    carry = jnp.zeros((1, columns), F32)
    attended = [jnp.zeros((HEADS, KEY_WIDTH), F32) for _ in range(tokens)]
    for block in range(cache_len // BLOCK - 1, -1, -1):
        span = slice(block * BLOCK, (block + 1) * BLOCK)
        score = lax.dot_general(key_ref[0, span, :], padded[0], NT, preferred_element_type=F32)
        for token in range(1, tokens):
            score = score + lax.dot_general(
                key_ref[token, span, :], padded[token], NT, preferred_element_type=F32
            )
        score = score * HEAD_DIM ** (-0.5) + bias
        spot = lax.broadcasted_iota(jnp.int32, score.shape, 0) + block * BLOCK
        alive = spot < live
        remain = -(jnp.maximum(score, 0.0) + jnp.log1p(jnp.exp(-jnp.abs(score))))
        remain = jnp.where(alive, remain, 0.0)
        high = remain.astype(BF16)
        low = (remain - high.astype(F32)).astype(BF16)
        inclusive = (
            jnp.dot(upper, high, preferred_element_type=F32)
            + jnp.dot(upper, low, preferred_element_type=F32)
            + carry
        )
        carry = inclusive[0:1, :]
        weight = jnp.where(alive, jnp.exp(score + inclusive), 0.0)
        weight = weight.T.astype(BF16)
        for token in range(tokens):
            attended[token] = attended[token] + jnp.dot(
                weight[token * HEADS : (token + 1) * HEADS, :],
                value_ref[token, span, :],
                preferred_element_type=F32,
            )

    own_row = lax.broadcasted_iota(jnp.int32, (HEADS, KEY_WIDTH), 0)
    own_col = lax.broadcasted_iota(jnp.int32, (HEADS, KEY_WIDTH), 1)
    keep = own_row // GROUP == own_col // HEAD_DIM
    for token in range(tokens):
        kept = jnp.where(keep, attended[token], 0.0)
        folded = kept[0:GROUP]
        for group in range(1, KV_HEADS):
            folded = folded + kept[group * GROUP : (group + 1) * GROUP]
        heads_scr[token] = folded
    for member in range(GROUP):
        piece = heads_scr[:, member, :].astype(BF16)
        for shard in range(shards):
            row_ref[shard, :, member * KEY_WIDTH : (member + 1) * KEY_WIDTH] = piece

    gate_row = lax.broadcasted_iota(jnp.int32, (tokens, 128), 0)
    gate_col = lax.broadcasted_iota(jnp.int32, (tokens, 128), 1)
    first = jnp.zeros((tokens, 128), jnp.int32)
    second = jnp.zeros((tokens, 128), jnp.int32)
    gap = jnp.zeros((tokens, 128), F32)
    for token in range(tokens):
        first = jnp.where(gate_row == token, routes_ref[0, token], first)
        second = jnp.where(gate_row == token, routes_ref[1, token], second)
        gap = jnp.where(gate_row == token, logits_ref[0, token] - logits_ref[1, token], gap)
    share = jnp.where(first == gate_col % 64, jax.nn.sigmoid(gap), 0.0)
    share = share + jnp.where(second == gate_col % 64, jax.nn.sigmoid(-gap), 0.0)
    share_high = share.astype(BF16).astype(F32)
    share = jnp.where(gate_col < 64, share_high, share - share_high).astype(BF16)
    for shard in range(shards):
        row_ref[shard, :, QUERY_WIDTH:] = share


def mix_kernel(rows_ref, tokens_ref, w_ref, mixed_ref):
    shards, tokens, width = tokens_ref.shape
    total = shards * tokens
    mixed = tokens_ref[...].astype(F32).reshape(total, width)
    rows = rows_ref[...].astype(F32).reshape(total, ROW_WIDTH).astype(BF16)
    for member in range(GROUP):
        pieces = []
        for group in range(KV_HEADS):
            head = group * GROUP + member
            pieces.append(w_ref[head * HEAD_DIM : (head + 1) * HEAD_DIM, :])
        weight = jnp.concatenate(pieces, axis=0)
        mixed = mixed + jnp.dot(
            rows[:, member * KEY_WIDTH : (member + 1) * KEY_WIDTH],
            weight,
            preferred_element_type=F32,
        )
    mixed = mixed.astype(BF16)
    for shard in range(shards):
        mixed_ref[shard] = mixed


def expert_kernel(expert_ref, mixed_ref, rows_ref, gain_ref, wg_ref, wu_ref, wd_ref, out_ref):
    total, features = mixed_ref.shape[-2], gain_ref.shape[1]
    shards, tokens = rows_ref.shape[:2]
    if len(mixed_ref.shape) == 3:
        mixed = jnp.concatenate([mixed_ref[s].astype(F32) for s in range(mixed_ref.shape[0])], axis=-1)
    else:
        mixed = mixed_ref[...].astype(F32)
    scale = lax.rsqrt(jnp.mean(mixed * mixed, axis=-1, keepdims=True) + EPSILON)
    expert_in = (mixed * scale * gain_ref[...]).astype(BF16)
    gates = rows_ref[:, :, QUERY_WIDTH:].astype(F32).reshape(total, 128)
    lane = lax.broadcasted_iota(jnp.int32, gates.shape, 1)
    gate = jnp.sum(jnp.where(lane % 64 == expert_ref[0], gates, 0.0), axis=-1, keepdims=True)
    size = wg_ref.shape[1]
    chunk = BLOCK if size % BLOCK == 0 else size
    result = jnp.zeros((total, features), F32)
    hidden = []
    for start in range(0, size, chunk):
        up = jnp.dot(expert_in, wu_ref[:, start : start + chunk], preferred_element_type=F32)
        value = jnp.dot(expert_in, wg_ref[:, start : start + chunk], preferred_element_type=F32)
        hidden.append((value / (1.0 + jnp.exp(-value)) * up * gate).astype(BF16))
    hidden = jnp.concatenate(hidden, axis=-1) if len(hidden) > 1 else hidden[0]
    for start in range(0, features, BLOCK):
        part = jnp.dot(hidden, wd_ref[:, start : start + BLOCK], preferred_element_type=F32)
        out_ref[:, :, start : start + BLOCK] = part.astype(BF16).reshape(shards, tokens, BLOCK)


def finish_kernel(parts_ref, mixed_ref, out_ref):
    total = mixed_ref[...].astype(F32)
    for shard in range(parts_ref.shape[0]):
        total = total + parts_ref[shard].astype(F32)
    out_ref[...] = total.astype(BF16)


def call(kernel, name, outs, specs, scratch=()):
    single = not isinstance(outs, tuple)
    return pl.pallas_call(
        kernel,
        name=name,
        out_shape=outs,
        in_specs=specs,
        out_specs=vmem_spec() if single else tuple(vmem_spec() for _ in outs),
        scratch_shapes=list(scratch),
        compiler_params=pltpu.CompilerParams(vmem_limit_bytes=20 << 20),
    )


def in_vmem(array):
    return pltpu.with_memory_space_constraint(array, VMEM)


def local(
    tokens,
    lengths,
    cache_key,
    cache_value,
    routes,
    route_logits,
    mix_gain,
    query_gain,
    key_gain,
    head_bias,
    w_query,
    w_key,
    w_value,
    w_out,
    ffn_gain,
    w_gate,
    w_up,
    w_down,
):
    shards = lax.axis_size("ep")
    me = lax.axis_index("ep")
    token_rows, width = tokens.shape
    share = width // shards
    all_rows = shards * token_rows
    exchange = functools.partial(lax.all_to_all, axis_name="ep", split_axis=0, concat_axis=0)
    shape = jax.ShapeDtypeStruct

    sliced = tokens.reshape(token_rows, shards, share).transpose(1, 0, 2)
    sliced = exchange(sliced)
    my_gain = lax.dynamic_slice_in_dim(mix_gain, me * share, share)[None, :]
    project_width = QUERY_WIDTH + 2 * KEY_WIDTH
    parts = call(
        project_kernel,
        "project",
        shape((shards, token_rows, project_width), BF16),
        [vmem_spec()] * 5,
    )(sliced, my_gain, w_query, w_key, w_value)
    parts = exchange(parts)

    rows, new_key, new_value = call(
        attend_kernel,
        "attend",
        (
            shape((shards, token_rows, ROW_WIDTH), BF16),
            shape((token_rows, KEY_WIDTH), BF16),
            shape((token_rows, KEY_WIDTH), BF16),
        ),
        [smem_spec()] * 4 + [vmem_spec()] * 6,
        [pltpu.VMEM((token_rows, GROUP, KEY_WIDTH), F32)],
    )(
        lengths,
        routes.T,
        route_logits.T,
        head_bias,
        parts,
        tokens,
        jnp.tile(query_gain, KV_HEADS)[None, :],
        jnp.tile(key_gain, KV_HEADS)[None, :],
        in_vmem(cache_key),
        in_vmem(cache_value),
    )
    rows = exchange(rows)

    mixed = call(
        mix_kernel,
        "mix",
        shape((shards, all_rows, share), BF16),
        [vmem_spec()] * 3,
    )(rows, sliced, w_out)
    mixed = exchange(mixed)

    ff_share = w_gate.shape[1]
    my_expert = (me // (FF // ff_share)).astype(jnp.int32).reshape(1)
    if share % 128:
        expert_rows = mixed.transpose(1, 0, 2).reshape(all_rows, width)
    else:
        expert_rows = mixed
    sums = call(
        expert_kernel,
        "expert",
        shape((shards, token_rows, width), BF16),
        [smem_spec()] + [vmem_spec()] * 6,
    )(
        my_expert,
        expert_rows,
        rows,
        ffn_gain[None, :],
        in_vmem(w_gate),
        in_vmem(w_up),
        in_vmem(w_down),
    )
    sums = exchange(sums)
    mine = lax.dynamic_slice_in_dim(mixed, me * token_rows, token_rows, 1)
    mine = mine.transpose(1, 0, 2).reshape(token_rows, width)
    output = call(
        finish_kernel, "finish", shape((token_rows, width), BF16), [vmem_spec()] * 2
    )(sums, mine)
    return output, new_key, new_value


def solution(mesh):
    return jax.shard_map(
        local,
        mesh=mesh,
        in_specs=(
            P(("grp", "ep"), None),
            P(("grp", "ep")),
            P(("grp", "ep"), None, None),
            P(("grp", "ep"), None, None),
            P(("grp", "ep"), None),
            P(("grp", "ep"), None),
            P(),
            P(),
            P(),
            P(),
            P("ep", None),
            P("ep", None),
            P("ep", None),
            P(None, "ep"),
            P(),
            P(None, "ep"),
            P(None, "ep"),
            P("ep", None),
        ),
        out_specs=(P(("grp", "ep"), None), P(("grp", "ep"), None), P(("grp", "ep"), None)),
        check_vma=False,
    )
```

time: 324 us -> 97.7 us (0.30)
  waiting for transfers between devices: 144 us -> 33.8 us
  other arithmetic: 87 us -> 0 us
  blocking collectives: 42.8 us -> 10.7 us
  matrix products: 25.7 us -> 0 us
  starting transfers between devices: 0.19 us -> 18 us
  between operations: 14.6 us -> 0.73 us
  local copies, waits for them, and re-layouts: 9.35 us -> 21.7 us
  Pallas kernels: 0 us -> 11.7 us
    unnamed x6 -> x0, waiting for transfers between devices: 88 us -> none
    another operation x3 -> x0, other arithmetic: 82.2 us -> none
    all_gather x4 -> x0, waiting for transfers between devices: 55.9 us -> none  [the longest x1 49.7 us: local(): lax.all_gather(w_query, 'ep', axis=0, tiled=True)]
    all_gather x2 -> x0, blocking collectives: 42.8 us -> none  [the longest x1 23.2 us: local(): lax.all_gather(route_weights(routes, route_logits), 'ep', axis=0, tiled=T...]
    all_to_all x0 -> x4, waiting for transfers between devices: none -> 33.8 us  [the longest x1 9.97 us: local(): mixed = exchange(mixed)]
    dot_general x8 -> x0, matrix products: 25.7 us -> none  [the longest x1 8.67 us: local(): jnp.dot(hidden, w_down, preferred_element_type=jnp.float32)]
    all_to_all x0 -> x4, starting transfers between devices: none -> 18 us  [the longest x1 7.43 us: local(): sliced = exchange(sliced)]
    unnamed x23 -> x32, local copies, waits for them, and re-layouts: 7.29 us -> 20.1 us
  transfers between devices with their start and end apart: 5 -> 4, of which waited for: 3 -> 4; matrix products, arithmetic and copies ran while one was open for 37% -> 2% of each run, Pallas kernels for 0% -> 0%
where the time goes in v1:
time: 97.7 us; the launch traced here: 96.7 us
  waiting for transfers between devices  33.8 us (35%)
  local copies, waits for them, and re-layouts  21.7 us (22%)
  starting transfers between devices  18 us (18%)
  Pallas kernels  11.7 us (12%)
  blocking collectives  10.7 us (11%)
    unnamed x32, local copies, waits for them, and re-layouts  20.1 us
    all_to_all x1, blocking collectives, local(): rows = exchange(rows)  10.7 us
    all_to_all x1, waiting for transfers between devices, local(): mixed = exchange(mixed)  9.97 us
    all_to_all x1, waiting for transfers between devices, local(): sums = exchange(sums)  9.95 us
    all_to_all x1, waiting for transfers between devices, local(): parts = exchange(parts)  7.44 us
    all_to_all x1, starting transfers between devices, local(): sliced = exchange(sliced)  7.43 us
    all_to_all x1, waiting for transfers between devices, local(): sliced = exchange(sliced)  6.41 us
    pallas_call x1, Pallas kernels, local(): call(expert_kernel, 'expert', shape((shards, token_rows, width), BF16), [...  4.78 us
  transfers between devices with their start and end apart: 4, of which 4 were waited for; matrix products, arithmetic and copies ran while one was open for 2% of the time, Pallas kernels for 0%

profile of v1, /device:TPU:0, one launch (start us, length us, event | category | flops | bytes accessed | tf_op | source)
XLA Modules:
  0.0 96.7 jit_solution(18059601912662942545)
XLA Ops:
  0.6 7.4 %all-to-all-start = ((bf16[16,4,128]{2,1,0:T(4,128)(2,1)}), bf16[16,4,128]{2,1,0:T(4,128)(2,1)S(1)}, u32[]{:S(2)}, u32[]{:S(2)}) async-start(bf16[16,4,128]{2,1,0:T(4,128)(2,1)} %bitcast.13), calls=%async_computation | async-start | bytes 32768 | tf_op jit(solution)/shard_map/all_to_all | solution.py:280
  8.2 6.4 %all-to-all-done.rows_ref.tokens_ref = bf16[16,4,128]{2,1,0:T(4,128)(2,1)S(1)} async-done(((bf16[16,4,128]{2,1,0:T(4,128)(2,1)}), bf16[16,4,128]{2,1,0:T(4,128)(2,1)S(1)}, u32[]{:S(2)}, u32[]{:S(2)}) %all-to-all-start) | async-done | bytes 16416 | tf_op jit(solution)/shard_map/all_to_all | solution.py:280
  14.6 0.9 copy-done.6
  15.5 0.8 copy-done.9
  16.4 0.8 copy-done.10
  17.2 0.9 project.1
  18.1 3.5 %all-to-all-start.1 = ((bf16[16,4,1536]{2,1,0:T(4,128)(2,1)}), bf16[16,4,1536]{2,1,0:T(4,128)(2,1)S(1)}, u32[]{:S(2)}, u32[]{:S(2)}) async-start(bf16[16,4,1536]{2,1,0:T(4,128)(2,1)} %project.1), calls=%async_computation.1 | async-start | bytes 393216 | tf_op jit(solution)/shard_map/all_to_all | solution.py:289
  21.6 0.7 tile.4
  22.3 0.1 broadcast_in_dim_tile.6.qgain_ref
  22.4 0.7 tile.5
  23.1 7.4 %all-to-all-done.1.parts_ref = bf16[16,4,1536]{2,1,0:T(4,128)(2,1)S(1)} async-done(((bf16[16,4,1536]{2,1,0:T(4,128)(2,1)}), bf16[16,4,1536]{2,1,0:T(4,128)(2,1)S(1)}, u32[]{:S(2)}, u32[]{:S(2)}) %all-to-all-start.1) | async-done | bytes 196640 | tf_op jit(solution)/shard_map/all_to_all | solution.py:289
  30.6 1.6 %copy-done.4 = bf16[4,1024,256]{2,1,0:T(8,128)(2,1)S(1)} copy-done((bf16[4,1024,256]{2,1,0:T(8,128)(2,1)S(1)}, bf16[4,1024,256]{2,1,0:T(8,128)(2,1)}, u32[]{:S(2)}) %copy-start.4) | copy-done | bytes 2097176
  32.1 1.6 %copy-done.5 = bf16[4,1024,256]{2,1,0:T(8,128)(2,1)S(1)} copy-done((bf16[4,1024,256]{2,1,0:T(8,128)(2,1)S(1)}, bf16[4,1024,256]{2,1,0:T(8,128)(2,1)}, u32[]{:S(2)}) %copy-start.5) | copy-done | bytes 2097176
  33.7 0.7 copy-done.8
  34.5 0.7 copy-done.12
  35.1 0.7 copy-done.13
  35.8 0.7 copy-done.14
  36.5 0.7 copy-done.15
  37.1 4.5 %attend.1 = (bf16[16,4,1152]{2,1,0:T(4,128)(2,1)S(1)}, bf16[4,256]{1,0:T(4,128)(2,1)}, bf16[4,256]{1,0:T(4,128)(2,1)}) custom-call(s32[4]{0:T(128)S(1)} %copy-done.14, s32[2,4]{1,0:T(2,128)S(1)} %bitcast.15, f32[2,4]{1,0:T(2,128)S(1)} %bitcast.16, f32[16]{0:T(128)S(1)} %copy-done.15, bf16[16,4,1536]{2,1,0:T(4,128)(2,1)S(1)} %all-to-all-done.1.parts_ref, ...), custom_call_target="tpu_custom_call" | custom-call | tf_op jit(solution)/shard_map/attend/pallas_call | solution.py:291
  41.6 10.7 %all_to_all.25.rows_ref = bf16[16,4,1152]{2,1,0:T(4,128)(2,1)S(1)} all-to-all(bf16[16,4,1152]{2,1,0:T(4,128)(2,1)S(1)} %get-tuple-element.6), channel_id=1, replica_groups=mesh['grp'=2,'ep'=16] {'ep'}, dimensions={0} | all-to-all | bytes 294912 | tf_op jit(solution)/shard_map/all_to_all | solution.py:313
  52.4 0.9 copy-done.7
  53.3 0.9 mix.1
  54.2 3.5 %all-to-all-start.3 = ((bf16[16,64,128]{2,1,0:T(8,128)(2,1)}), bf16[16,64,128]{2,1,0:T(8,128)(2,1)S(1)}, u32[]{:S(2)}, u32[]{:S(2)}) async-start(bf16[16,64,128]{2,1,0:T(8,128)(2,1)} %mix.1), calls=%async_computation.3 | async-start | bytes 524288 | tf_op jit(solution)/shard_map/all_to_all | solution.py:321
  57.8 10.0 %all-to-all-done.3.mixed_ref = bf16[16,64,128]{2,1,0:T(8,128)(2,1)S(1)} async-done(((bf16[16,64,128]{2,1,0:T(8,128)(2,1)}), bf16[16,64,128]{2,1,0:T(8,128)(2,1)S(1)}, u32[]{:S(2)}, u32[]{:S(2)}) %all-to-all-start.3) | async-done | bytes 262176 | tf_op jit(solution)/shard_map/all_to_all | solution.py:321
  67.8 3.1 %copy-done.1 = bf16[2048,1792]{1,0:T(8,128)(2,1)S(1)} copy-done((bf16[2048,1792]{1,0:T(8,128)(2,1)S(1)}, bf16[2048,1792]{1,0:T(8,128)(2,1)}, u32[]{:S(2)}) %copy-start.1) | copy-done | bytes 7340056
  70.8 3.1 %copy-done.2 = bf16[2048,1792]{1,0:T(8,128)(2,1)S(1)} copy-done((bf16[2048,1792]{1,0:T(8,128)(2,1)S(1)}, bf16[2048,1792]{1,0:T(8,128)(2,1)}, u32[]{:S(2)}) %copy-start.2) | copy-done | bytes 7340056
  73.9 3.1 %copy-done.3 = bf16[1792,2048]{1,0:T(8,128)(2,1)S(1)} copy-done((bf16[1792,2048]{1,0:T(8,128)(2,1)S(1)}, bf16[1792,2048]{1,0:T(8,128)(2,1)}, u32[]{:S(2)}) %copy-start.3) | copy-done | bytes 7340056
  77.0 0.7 copy-done.11
  77.7 4.8 %expert.1 = bf16[16,4,2048]{2,1,0:T(4,128)(2,1)} custom-call(s32[1]{0:T(128)} %bitcast.expert_ref, bf16[16,64,128]{2,1,0:T(8,128)(2,1)S(1)} %all-to-all-done.3.mixed_ref, bf16[16,4,1152]{2,1,0:T(4,128)(2,1)S(1)} %all_to_all.25.rows_ref, f32[1,2048]{1,0:T(1,128)S(1)} %bitcast.14, bf16[2048,1792]{1,0:T(8,128)(2,1)S(1)} %copy-done.1, ...), custom_call_target="tpu_custom_call" | custom-call | tf_op jit(solution)/shard_map/expert/pallas_call | solution.py:329
  82.5 3.5 %all-to-all-start.4 = ((bf16[16,4,2048]{2,1,0:T(4,128)(2,1)}), bf16[16,4,2048]{2,1,0:T(4,128)(2,1)S(1)}, u32[]{:S(2)}, u32[]{:S(2)}) async-start(bf16[16,4,2048]{2,1,0:T(4,128)(2,1)} %expert.1), calls=%async_computation.4 | async-start | bytes 524288 | tf_op jit(solution)/shard_map/all_to_all | solution.py:343
  86.1 9.9 %all-to-all-done.4.parts_ref = bf16[16,4,2048]{2,1,0:T(4,128)(2,1)S(1)} async-done(((bf16[16,4,2048]{2,1,0:T(4,128)(2,1)}), bf16[16,4,2048]{2,1,0:T(4,128)(2,1)S(1)}, u32[]{:S(2)}, u32[]{:S(2)}) %all-to-all-start.4) | async-done | bytes 262176 | tf_op jit(solution)/shard_map/all_to_all | solution.py:343
  96.0 0.7 finish.1
  (20 shorter events, 0.2 us)
Async XLA Ops:
  0.6 7.5 %copy-start = (f32[2048]{0:T(1024)S(1)}, f32[2048]{0:T(1024)}, u32[]{:S(2)}) copy-start(f32[2048]{0:T(1024)} %param.24) | copy-start | bytes 24580
  0.6 13.9 %all-to-all-start = ((bf16[16,4,128]{2,1,0:T(4,128)(2,1)}), bf16[16,4,128]{2,1,0:T(4,128)(2,1)S(1)}, u32[]{:S(2)}, u32[]{:S(2)}) async-start(bf16[16,4,128]{2,1,0:T(4,128)(2,1)} %bitcast.13), calls=%async_computation | async-start | bytes 32768 | tf_op jit(solution)/shard_map/all_to_all | solution.py:280
  14.6 1.0 copy-start.6
  15.5 0.8 copy-start.9
  16.4 0.8 copy-start.10
  18.1 12.5 %all-to-all-start.1 = ((bf16[16,4,1536]{2,1,0:T(4,128)(2,1)}), bf16[16,4,1536]{2,1,0:T(4,128)(2,1)S(1)}, u32[]{:S(2)}, u32[]{:S(2)}) async-start(bf16[16,4,1536]{2,1,0:T(4,128)(2,1)} %project.1), calls=%async_computation.1 | async-start | bytes 393216 | tf_op jit(solution)/shard_map/all_to_all | solution.py:289
  30.6 1.6 %copy-start.4 = (bf16[4,1024,256]{2,1,0:T(8,128)(2,1)S(1)}, bf16[4,1024,256]{2,1,0:T(8,128)(2,1)}, u32[]{:S(2)}) copy-start(bf16[4,1024,256]{2,1,0:T(8,128)(2,1)} %key_ref.1) | copy-start | bytes 6291460
  32.1 1.6 %copy-start.5 = (bf16[4,1024,256]{2,1,0:T(8,128)(2,1)S(1)}, bf16[4,1024,256]{2,1,0:T(8,128)(2,1)}, u32[]{:S(2)}) copy-start(bf16[4,1024,256]{2,1,0:T(8,128)(2,1)} %value_ref.1) | copy-start | bytes 6291460
  33.7 0.7 copy-start.8
  34.5 0.7 copy-start.12
  35.1 0.7 copy-start.13
  35.8 0.7 copy-start.14
  36.5 0.7 copy-start.15
  52.4 1.0 copy-start.7
  54.2 13.5 %all-to-all-start.3 = ((bf16[16,64,128]{2,1,0:T(8,128)(2,1)}), bf16[16,64,128]{2,1,0:T(8,128)(2,1)S(1)}, u32[]{:S(2)}, u32[]{:S(2)}) async-start(bf16[16,64,128]{2,1,0:T(8,128)(2,1)} %mix.1), calls=%async_computation.3 | async-start | bytes 524288 | tf_op jit(solution)/shard_map/all_to_all | solution.py:321
  67.8 3.1 %copy-start.1 = (bf16[2048,1792]{1,0:T(8,128)(2,1)S(1)}, bf16[2048,1792]{1,0:T(8,128)(2,1)}, u32[]{:S(2)}) copy-start(bf16[2048,1792]{1,0:T(8,128)(2,1)} %wg_ref.1) | copy-start | bytes 22020100
  70.8 3.1 %copy-start.2 = (bf16[2048,1792]{1,0:T(8,128)(2,1)S(1)}, bf16[2048,1792]{1,0:T(8,128)(2,1)}, u32[]{:S(2)}) copy-start(bf16[2048,1792]{1,0:T(8,128)(2,1)} %wu_ref.1) | copy-start | bytes 22020100
  73.9 3.1 %copy-start.3 = (bf16[1792,2048]{1,0:T(8,128)(2,1)S(1)}, bf16[1792,2048]{1,0:T(8,128)(2,1)}, u32[]{:S(2)}) copy-start(bf16[1792,2048]{1,0:T(8,128)(2,1)} %wd_ref.1) | copy-start | bytes 22020100
  77.0 0.7 copy-start.11
  82.5 13.5 %all-to-all-start.4 = ((bf16[16,4,2048]{2,1,0:T(4,128)(2,1)}), bf16[16,4,2048]{2,1,0:T(4,128)(2,1)S(1)}, u32[]{:S(2)}, u32[]{:S(2)}) async-start(bf16[16,4,2048]{2,1,0:T(4,128)(2,1)} %expert.1), calls=%async_computation.4 | async-start | bytes 524288 | tf_op jit(solution)/shard_map/all_to_all | solution.py:343

commit v2 on v1

v2 whole, which is shorter than its diff:
```python
import functools

import jax
import jax.numpy as jnp
from jax import lax
from jax.experimental import pallas as pl
from jax.experimental.pallas import tpu as pltpu
from jax.sharding import PartitionSpec as P

HEADS = 16
KV_HEADS = 4
HEAD_DIM = 64
FF = 7168
EXPERTS = 4
EPSILON = 1e-06

GROUP = HEADS // KV_HEADS
KEY_WIDTH = KV_HEADS * HEAD_DIM
QUERY_WIDTH = HEADS * HEAD_DIM
ROW_WIDTH = QUERY_WIDTH + 128
BLOCK = 256
F32 = jnp.float32
BF16 = jnp.bfloat16
VMEM = pltpu.VMEM
NT = (((1,), (1,)), ((), ()))


def vmem_spec():
    return pl.BlockSpec(memory_space=VMEM)


def smem_spec():
    return pl.BlockSpec(memory_space=pltpu.SMEM)


def stage_kernel(
    lengths_hbm,
    routes_hbm,
    logits_hbm,
    bias_hbm,
    qgain_hbm,
    kgain_hbm,
    mix_gain_hbm,
    ffn_gain_hbm,
    tokens_hbm,
    wq_hbm,
    wk_hbm,
    wv_hbm,
    w_out_hbm,
    key_hbm,
    my_gain_ref,
    scale_ref,
    column_ref,
    head_gain_ref,
    share_ref,
    ffn_gain_ref,
    w_in_ref,
    w_out_ref,
    key_ref,
    lengths_scr,
    routes_scr,
    logits_scr,
    bias_scr,
    head_gain_scr,
    mix_gain_scr,
    tokens_scr,
    sems,
):
    tokens = tokens_hbm.shape[0]
    small = [
        (lengths_hbm, lengths_scr),
        (routes_hbm, routes_scr),
        (logits_hbm, logits_scr),
        (bias_hbm, bias_scr),
        (qgain_hbm, head_gain_scr.at[0]),
        (kgain_hbm, head_gain_scr.at[1]),
        (mix_gain_hbm, mix_gain_scr),
        (tokens_hbm, tokens_scr),
    ]
    large = [(ffn_gain_hbm, ffn_gain_ref)]
    start = 0
    for source in (wq_hbm, wk_hbm, wv_hbm):
        large.append((source, w_in_ref.at[:, start : start + source.shape[1]]))
        start += source.shape[1]
    large += [
        (w_out_hbm, w_out_ref),
        (key_hbm, key_ref),
    ]
    copies = [
        pltpu.make_async_copy(source, target, sems.at[index])
        for index, (source, target) in enumerate(small + large)
    ]
    for copy in copies:
        copy.start()
    for copy in copies[: len(small)]:
        copy.wait()

    me = lax.axis_index("ep")
    my_gain_ref[...] = mix_gain_scr[pl.ds(me, 1), :]
    own = tokens_scr[...].astype(F32)
    token_scale = lax.rsqrt(jnp.mean(own * own, axis=-1, keepdims=True) + EPSILON)
    scale_ref[...] = jnp.broadcast_to(token_scale, scale_ref.shape)
    for index in range(2):
        head_gain_ref[index : index + 1, :] = jnp.concatenate(
            [head_gain_scr[index]] * KV_HEADS, axis=-1
        )

    column = lax.broadcasted_iota(jnp.int32, (1, tokens * HEADS), 1)
    live = jnp.zeros(column.shape, jnp.int32)
    bias = jnp.zeros(column.shape, F32)
    for token in range(tokens):
        live = jnp.where(column // HEADS == token, lengths_scr[token], live)
    for head in range(HEADS):
        bias = jnp.where(column % HEADS == head, bias_scr[head], bias)
    column_ref[0:1, :] = live.astype(F32)
    column_ref[1:2, :] = bias

    row = lax.broadcasted_iota(jnp.int32, share_ref.shape, 0)
    lane = lax.broadcasted_iota(jnp.int32, share_ref.shape, 1)
    first = jnp.zeros(share_ref.shape, jnp.int32)
    second = jnp.zeros(share_ref.shape, jnp.int32)
    gap = jnp.zeros(share_ref.shape, F32)
    for token in range(tokens):
        first = jnp.where(row == token, routes_scr[0, token], first)
        second = jnp.where(row == token, routes_scr[1, token], second)
        gap = jnp.where(row == token, logits_scr[0, token] - logits_scr[1, token], gap)
    share = jnp.where(first == lane % 64, jax.nn.sigmoid(gap), 0.0)
    share = share + jnp.where(second == lane % 64, jax.nn.sigmoid(-gap), 0.0)
    high = share.astype(BF16).astype(F32)
    share_ref[...] = jnp.where(lane < 64, high, share - high).astype(BF16)
    for copy in copies[len(small) :]:
        copy.wait()


def project_kernel(rows_ref, gain_ref, w_ref, out_ref):
    shards, tokens, width = rows_ref.shape
    rows = rows_ref[...].astype(F32).reshape(shards * tokens, width)
    scaled = (rows * gain_ref[...]).astype(BF16)
    part = jnp.dot(scaled, w_ref[...], preferred_element_type=F32)
    out_ref[...] = part.astype(BF16).reshape(out_ref.shape)


def attend_kernel(
    parts_ref,
    scale_ref,
    column_ref,
    head_gain_ref,
    share_ref,
    key_ref,
    value_hbm,
    row_ref,
    new_key_ref,
    new_value_ref,
    heads_scr,
    value_ref,
    sem,
):
    fetch = pltpu.make_async_copy(value_hbm, value_ref, sem)
    fetch.start()
    shards, tokens, _ = parts_ref.shape
    cache_len = key_ref.shape[1]
    columns = tokens * HEADS

    total = parts_ref[0].astype(F32)
    for shard in range(1, shards):
        total = total + parts_ref[shard].astype(F32)
    total = total * scale_ref[:, 0:1]
    fresh_key = total[:, QUERY_WIDTH : QUERY_WIDTH + KEY_WIDTH]
    new_value_ref[...] = total[:, QUERY_WIDTH + KEY_WIDTH :].astype(BF16)

    lane = lax.broadcasted_iota(jnp.int32, (tokens, KEY_WIDTH), 1)
    squares = fresh_key * fresh_key
    key_scale = jnp.zeros_like(fresh_key)
    for head in range(KV_HEADS):
        mine = lane // HEAD_DIM == head
        mean = jnp.sum(jnp.where(mine, squares, 0.0), axis=-1, keepdims=True) / HEAD_DIM
        key_scale = jnp.where(mine, lax.rsqrt(mean + EPSILON), key_scale)
    new_key_ref[...] = (fresh_key * key_scale * head_gain_ref[1:2, :]).astype(BF16)

    for member in range(GROUP):
        pieces = []
        for group in range(KV_HEADS):
            head = group * GROUP + member
            pieces.append(total[:, head * HEAD_DIM : (head + 1) * HEAD_DIM])
        heads_scr[:, member, :] = jnp.concatenate(pieces, axis=-1)
    stacked = []
    for token in range(tokens):
        stacked += [heads_scr[token]] * KV_HEADS
    query = jnp.concatenate(stacked, axis=0)
    row = lax.broadcasted_iota(jnp.int32, query.shape, 0)
    col = lax.broadcasted_iota(jnp.int32, query.shape, 1)
    query = jnp.where(row % HEADS // GROUP == col // HEAD_DIM, query, 0.0)
    query_mean = jnp.sum(query * query, axis=-1, keepdims=True) / HEAD_DIM
    query = query * lax.rsqrt(query_mean + EPSILON) * head_gain_ref[0:1, :]
    query = query.astype(BF16).astype(F32)
    padded = [
        jnp.where(row // HEADS == token, query, 0.0).astype(BF16) for token in range(tokens)
    ]

    live = column_ref[0:1, :]
    bias = column_ref[1:2, :]
    upper = (
        lax.broadcasted_iota(jnp.int32, (BLOCK, BLOCK), 1)
        >= lax.broadcasted_iota(jnp.int32, (BLOCK, BLOCK), 0)
    ).astype(F32).astype(BF16)
    carry = jnp.zeros((1, columns), F32)
    attended = [jnp.zeros((HEADS, KEY_WIDTH), F32) for _ in range(tokens)]
    for block in range(cache_len // BLOCK - 1, -1, -1):
        span = slice(block * BLOCK, (block + 1) * BLOCK)
        score = lax.dot_general(key_ref[0, span, :], padded[0], NT, preferred_element_type=F32)
        for token in range(1, tokens):
            score = score + lax.dot_general(
                key_ref[token, span, :], padded[token], NT, preferred_element_type=F32
            )
        score = score * HEAD_DIM ** (-0.5) + bias
        spot = lax.broadcasted_iota(jnp.int32, score.shape, 0) + block * BLOCK
        alive = spot.astype(F32) < live
        remain = -(jnp.maximum(score, 0.0) + jnp.log1p(jnp.exp(-jnp.abs(score))))
        remain = jnp.where(alive, remain, 0.0)
        high = remain.astype(BF16)
        low = (remain - high.astype(F32)).astype(BF16)
        inclusive = (
            jnp.dot(upper, high, preferred_element_type=F32)
            + jnp.dot(upper, low, preferred_element_type=F32)
            + carry
        )
        carry = inclusive[0:1, :]
        weight = jnp.where(alive, jnp.exp(score + inclusive), 0.0)
        weight = weight.T.astype(BF16)
        if block == cache_len // BLOCK - 1:
            fetch.wait()
        for token in range(tokens):
            attended[token] = attended[token] + jnp.dot(
                weight[token * HEADS : (token + 1) * HEADS, :],
                value_ref[token, span, :],
                preferred_element_type=F32,
            )

    own_row = lax.broadcasted_iota(jnp.int32, (HEADS, KEY_WIDTH), 0)
    own_col = lax.broadcasted_iota(jnp.int32, (HEADS, KEY_WIDTH), 1)
    keep = own_row // GROUP == own_col // HEAD_DIM
    for token in range(tokens):
        kept = jnp.where(keep, attended[token], 0.0)
        folded = kept[0:GROUP]
        for group in range(1, KV_HEADS):
            folded = folded + kept[group * GROUP : (group + 1) * GROUP]
        heads_scr[token] = folded
    for member in range(GROUP):
        piece = heads_scr[:, member, :].astype(BF16)
        for shard in range(shards):
            row_ref[shard, :, member * KEY_WIDTH : (member + 1) * KEY_WIDTH] = piece

    for shard in range(shards):
        row_ref[shard, :, QUERY_WIDTH:] = share_ref[...]


def mix_kernel(rows_ref, tokens_ref, w_ref, mixed_ref):
    shards, tokens, width = tokens_ref.shape
    total = shards * tokens
    mixed = tokens_ref[...].astype(F32).reshape(total, width)
    rows = rows_ref[...].astype(F32).reshape(total, ROW_WIDTH).astype(BF16)
    for member in range(GROUP):
        pieces = []
        for group in range(KV_HEADS):
            head = group * GROUP + member
            pieces.append(w_ref[head * HEAD_DIM : (head + 1) * HEAD_DIM, :])
        weight = jnp.concatenate(pieces, axis=0)
        mixed = mixed + jnp.dot(
            rows[:, member * KEY_WIDTH : (member + 1) * KEY_WIDTH],
            weight,
            preferred_element_type=F32,
        )
    mixed = mixed.astype(BF16)
    for shard in range(shards):
        mixed_ref[shard] = mixed


def chunk_of(size):
    return BLOCK if size % BLOCK == 0 else size


def expert_kernel(
    mixed_ref,
    rows_ref,
    gain_ref,
    wg_hbm,
    wu_hbm,
    wd_hbm,
    out_ref,
    own_ref,
    wg_ref,
    wu_ref,
    wd_ref,
    sems,
):
    size = wg_ref.shape[1]
    chunk = chunk_of(size)
    steps = size // chunk
    copies = []
    for step in range(steps):
        span = slice(step * chunk, (step + 1) * chunk)
        for index, (source, target) in enumerate(((wg_hbm, wg_ref), (wu_hbm, wu_ref))):
            copies.append(
                pltpu.make_async_copy(
                    source.at[:, span], target.at[:, span], sems.at[index, step]
                )
            )
    for step in range(steps):
        span = slice(step * chunk, (step + 1) * chunk)
        copies.append(
            pltpu.make_async_copy(wd_hbm.at[span, :], wd_ref.at[span, :], sems.at[2, step])
        )
    for copy in copies:
        copy.start()

    total, features = mixed_ref.shape[-2], gain_ref.shape[1]
    shards, tokens = rows_ref.shape[:2]
    if len(mixed_ref.shape) == 3:
        mixed = jnp.concatenate([mixed_ref[s].astype(F32) for s in range(mixed_ref.shape[0])], axis=-1)
    else:
        mixed = mixed_ref[...].astype(F32)
    me = lax.axis_index("ep")
    picked = lax.broadcasted_iota(jnp.int32, (tokens, total), 1) - me * tokens
    picked = picked == lax.broadcasted_iota(jnp.int32, (tokens, total), 0)
    own_ref[...] = jnp.dot(
        picked.astype(F32).astype(BF16), mixed.astype(BF16), preferred_element_type=F32
    )
    scale = lax.rsqrt(jnp.mean(mixed * mixed, axis=-1, keepdims=True) + EPSILON)
    expert_in = (mixed * scale * gain_ref[...]).astype(BF16)
    gates = rows_ref[:, :, QUERY_WIDTH:].astype(F32).reshape(total, 128)
    lane = lax.broadcasted_iota(jnp.int32, gates.shape, 1)
    gate = jnp.where(lane % 64 == me // (FF // size), gates, 0.0)
    gate = jnp.sum(gate, axis=-1, keepdims=True)
    hidden = []
    for step in range(steps):
        span = slice(step * chunk, (step + 1) * chunk)
        copies[2 * step].wait()
        value = jnp.dot(expert_in, wg_ref[:, span], preferred_element_type=F32)
        copies[2 * step + 1].wait()
        up = jnp.dot(expert_in, wu_ref[:, span], preferred_element_type=F32)
        hidden.append((value / (1.0 + jnp.exp(-value)) * up * gate).astype(BF16))
    result = None
    for step in range(steps):
        span = slice(step * chunk, (step + 1) * chunk)
        copies[2 * steps + step].wait()
        part = jnp.dot(hidden[step], wd_ref[span, :], preferred_element_type=F32)
        result = part if result is None else result + part
    out_ref[...] = result.astype(BF16).reshape(out_ref.shape)


def finish_kernel(parts_ref, mixed_ref, out_ref):
    total = mixed_ref[...]
    for shard in range(parts_ref.shape[0]):
        total = total + parts_ref[shard].astype(F32)
    out_ref[...] = total.astype(BF16)


def call(kernel, name, outs, specs, scratch=(), limit=20):
    return pl.pallas_call(
        kernel,
        name=name,
        out_shape=outs,
        in_specs=specs,
        out_specs=jax.tree.map(lambda _: vmem_spec(), outs),
        scratch_shapes=list(scratch),
        compiler_params=pltpu.CompilerParams(vmem_limit_bytes=limit << 20),
    )


def hbm_spec():
    return pl.BlockSpec(memory_space=pltpu.HBM)


def in_hbm(array):
    return pltpu.with_memory_space_constraint(array, pltpu.HBM)


def local(
    tokens,
    lengths,
    cache_key,
    cache_value,
    routes,
    route_logits,
    mix_gain,
    query_gain,
    key_gain,
    head_bias,
    w_query,
    w_key,
    w_value,
    w_out,
    ffn_gain,
    w_gate,
    w_up,
    w_down,
):
    shards = lax.axis_size("ep")
    token_rows, width = tokens.shape
    share = width // shards
    all_rows = shards * token_rows
    exchange = functools.partial(lax.all_to_all, axis_name="ep", split_axis=0, concat_axis=0)
    kept = pltpu.VMEM
    project_width = QUERY_WIDTH + 2 * KEY_WIDTH

    with jax.named_scope("slices"):
        sliced = exchange(tokens.reshape(token_rows, shards, share).transpose(1, 0, 2))
    staged = [
        lengths,
        routes.T,
        route_logits.T,
        head_bias,
        query_gain[None, :],
        key_gain[None, :],
        mix_gain.reshape(shards, share),
        ffn_gain[None, :],
        tokens,
        w_query,
        w_key,
        w_value,
        w_out,
        cache_key,
    ]
    my_gain, scale, column, head_gain, gates, ffn_row, w_in, w_mix, key = call(
        stage_kernel,
        "stage",
        (
            kept((1, share), F32),
            kept((token_rows, 128), F32),
            kept((2, token_rows * HEADS), F32),
            kept((2, KEY_WIDTH), F32),
            kept((token_rows, 128), BF16),
            kept((1, width), F32),
            kept((share, project_width), BF16),
            kept(w_out.shape, BF16),
            kept(cache_key.shape, BF16),
        ),
        [hbm_spec()] * len(staged),
        [
            pltpu.SMEM(lengths.shape, jnp.int32),
            pltpu.SMEM((2, token_rows), jnp.int32),
            pltpu.SMEM((2, token_rows), F32),
            pltpu.SMEM(head_bias.shape, F32),
            pltpu.VMEM((2, 1, HEAD_DIM), F32),
            pltpu.VMEM((shards, share), F32),
            pltpu.VMEM(tokens.shape, BF16),
            pltpu.SemaphoreType.DMA((len(staged),)),
        ],
        limit=4,
    )(*[in_hbm(array) for array in staged])
    parts = call(
        project_kernel,
        "project",
        kept((shards, token_rows, project_width), BF16),
        [vmem_spec()] * 3,
        limit=8,
    )(sliced, my_gain, w_in)
    with jax.named_scope("partial"):
        parts = exchange(parts)

    rows, new_key, new_value = call(
        attend_kernel,
        "attend",
        (
            kept((shards, token_rows, ROW_WIDTH), BF16),
            jax.ShapeDtypeStruct((token_rows, KEY_WIDTH), BF16),
            jax.ShapeDtypeStruct((token_rows, KEY_WIDTH), BF16),
        ),
        [vmem_spec()] * 6 + [hbm_spec()],
        [
            pltpu.VMEM((token_rows, GROUP, KEY_WIDTH), F32),
            pltpu.VMEM(cache_value.shape, BF16),
            pltpu.SemaphoreType.DMA,
        ],
    )(parts, scale, column, head_gain, gates, key, in_hbm(cache_value))
    with jax.named_scope("rows"):
        rows = exchange(rows)

    mixed = call(
        mix_kernel,
        "mix",
        kept((shards, all_rows, share), BF16),
        [vmem_spec()] * 3,
        limit=8,
    )(rows, sliced, w_mix)
    with jax.named_scope("mixed"):
        mixed = exchange(mixed)

    if share % 128:
        expert_rows = mixed.transpose(1, 0, 2).reshape(all_rows, width)
    else:
        expert_rows = mixed
    sums, own = call(
        expert_kernel,
        "expert",
        (kept((shards, token_rows, width), BF16), kept((token_rows, width), F32)),
        [vmem_spec()] * 3 + [hbm_spec()] * 3,
        [
            pltpu.VMEM(w_gate.shape, BF16),
            pltpu.VMEM(w_up.shape, BF16),
            pltpu.VMEM(w_down.shape, BF16),
            pltpu.SemaphoreType.DMA((3, w_gate.shape[1] // chunk_of(w_gate.shape[1]))),
        ],
        limit=40,
    )(expert_rows, rows, ffn_row, in_hbm(w_gate), in_hbm(w_up), in_hbm(w_down))
    with jax.named_scope("sums"):
        sums = exchange(sums)
    output = call(
        finish_kernel,
        "finish",
        jax.ShapeDtypeStruct((token_rows, width), BF16),
        [vmem_spec()] * 2,
        limit=8,
    )(sums, own)
    return output, new_key, new_value


def solution(mesh):
    return jax.shard_map(
        local,
        mesh=mesh,
        in_specs=(
            P(("grp", "ep"), None),
            P(("grp", "ep")),
            P(("grp", "ep"), None, None),
            P(("grp", "ep"), None, None),
            P(("grp", "ep"), None),
            P(("grp", "ep"), None),
            P(),
            P(),
            P(),
            P(),
            P("ep", None),
            P("ep", None),
            P("ep", None),
            P(None, "ep"),
            P(),
            P(None, "ep"),
            P(None, "ep"),
            P("ep", None),
        ),
        out_specs=(P(("grp", "ep"), None), P(("grp", "ep"), None), P(("grp", "ep"), None)),
        check_vma=False,
    )
```

time: 97.7 us -> 77.5 us (0.79)
  blocking collectives: 10.7 us -> 47.6 us
  waiting for transfers between devices: 33.8 us -> 4.45 us
  local copies, waits for them, and re-layouts: 21.7 us -> 0 us
  starting transfers between devices: 18 us -> 7.42 us
  Pallas kernels: 11.7 us -> 16.9 us
    all_to_all x0 -> x3, blocking collectives: none -> 36.9 us  [the longest x1 12.7 us: local(): sums = exchange(sums)]
    all_to_all x4 -> x1, waiting for transfers between devices: 33.8 us -> 4.45 us  [local(): exchange(tokens.reshape(token_rows, shards, share).transpose(1, 0, 2))]
    unnamed x32 -> x0, local copies, waits for them, and re-layouts: 20.1 us -> none
    all_to_all x4 -> x1, starting transfers between devices: 18 us -> 7.42 us  [local(): exchange(tokens.reshape(token_rows, shards, share).transpose(1, 0, 2))]
    pallas_call x5 -> x6, Pallas kernels: 11.7 us -> 16.9 us  [the longest x1 8.95 us: local(): call(expert_kernel, 'expert', (kept((shards, token_rows, width), BF16), k...]
    another operation x4 -> x0, local copies, waits for them, and re-layouts: 1.48 us -> none  [the longest x2 0.74 us: local(): jnp.tile(query_gain, KV_HEADS)[None, :]]
  transfers between devices with their start and end apart: 4 -> 1, of which waited for: 4 -> 1; matrix products, arithmetic and copies ran while one was open for 2% -> 0% of each run, Pallas kernels for 0% -> 3%
where the time goes in v2:
time: 77.5 us; the launch traced here: 77.1 us
  blocking collectives  47.6 us (61%)
  Pallas kernels  16.9 us (22%)
  starting transfers between devices  7.42 us (10%)
  waiting for transfers between devices  4.45 us (6%)
    all_to_all x1, blocking collectives, local(): sums = exchange(sums)  12.7 us
    all_to_all x1, blocking collectives, local(): mixed = exchange(mixed)  12.6 us
    all_to_all x1, blocking collectives, local(): parts = exchange(parts)  11.6 us
    all_to_all x1, blocking collectives, local(): rows = exchange(rows)  10.8 us
    pallas_call x1, Pallas kernels, local(): call(expert_kernel, 'expert', (kept((shards, token_rows, width), BF16), k...  8.95 us
    all_to_all x1, starting transfers between devices, local(): exchange(tokens.reshape(token_rows, shards, share).transpose(1, 0, 2))  7.42 us
    pallas_call x1, Pallas kernels, local(): call(attend_kernel, 'attend', (kept((shards, token_rows, ROW_WIDTH), BF16...  4.87 us
    all_to_all x1, waiting for transfers between devices, local(): exchange(tokens.reshape(token_rows, shards, share).transpose(1, 0, 2))  4.45 us
  transfers between devices with their start and end apart: 1, of which 1 were waited for; matrix products, arithmetic and copies ran while one was open for 0% of the time, Pallas kernels for 3%

profile of v2, /device:TPU:0, one launch (start us, length us, event | category | flops | bytes accessed | tf_op | source)
XLA Modules:
  0.0 77.1 jit_solution(10703035404586433528)
XLA Ops:
  0.6 7.4 %all-to-all-start = ((bf16[16,4,128]{2,1,0:T(4,128)(2,1)}), bf16[16,4,128]{2,1,0:T(4,128)(2,1)S(1)}, u32[]{:S(2)}, u32[]{:S(2)}) async-start(bf16[16,4,128]{2,1,0:T(4,128)(2,1)} %bitcast.9), calls=%async_computation | async-start | bytes 32768 | tf_op jit(solution)/shard_map/slices/all_to_all | solution.py:407
  8.1 2.0 %stage.1 = (f32[1,128]{1,0:T(1,128)S(1)}, f32[4,128]{1,0:T(4,128)S(1)}, f32[2,64]{1,0:T(2,128)S(1)}, f32[2,256]{1,0:T(2,128)S(1)}, bf16[4,128]{1,0:T(4,128)(2,1)...) custom-call(s32[4]{0:T(128)} %lengths_hbm.1, ...), custom_call_target="tpu_custom_call" | custom-call | tf_op jit(solution)/shard_map/stage/pallas_call | solution.py:424
  10.1 4.5 %all-to-all-done.rows_ref.tokens_ref = bf16[16,4,128]{2,1,0:T(4,128)(2,1)S(1)} async-done(((bf16[16,4,128]{2,1,0:T(4,128)(2,1)}), bf16[16,4,128]{2,1,0:T(4,128)(2,1)S(1)}, u32[]{:S(2)}, u32[]{:S(2)}) %all-to-all-start) | async-done | bytes 16416 | tf_op jit(solution)/shard_map/slices/all_to_all | solution.py:407
  14.6 0.2 project.1
  14.8 11.6 %all_to_all.25.parts_ref = bf16[16,4,1536]{2,1,0:T(4,128)(2,1)S(1)} all-to-all(bf16[16,4,1536]{2,1,0:T(4,128)(2,1)S(1)} %project.1), channel_id=1, replica_groups=mesh['grp'=2,'ep'=16] {'ep'}, dimensions={0} | all-to-all | bytes 393216 | tf_op jit(solution)/shard_map/partial/all_to_all | solution.py:459
  26.3 4.9 %attend.1 = (bf16[16,4,1152]{2,1,0:T(4,128)(2,1)S(1)}, bf16[4,256]{1,0:T(4,128)(2,1)}, bf16[4,256]{1,0:T(4,128)(2,1)}) custom-call(bf16[16,4,1536]{2,1,0:T(4,128)(2,1)S(1)} %all_to_all.25.parts_ref, f32[4,128]{1,0:T(4,128)S(1)} %get-tuple-element.19.scale_ref, f32[2,64]{1,0:T(2,128)S(1)} %get-tuple-element.20.column_ref, ...), custom_call_target="tpu_custom_call" | custom-call | tf_op jit(solution)/shard_map/attend/pallas_call | solution.py:461
  31.2 10.8 %all_to_all.26.rows_ref = bf16[16,4,1152]{2,1,0:T(4,128)(2,1)S(1)} all-to-all(bf16[16,4,1152]{2,1,0:T(4,128)(2,1)S(1)} %get-tuple-element.24), channel_id=1, replica_groups=mesh['grp'=2,'ep'=16] {'ep'}, dimensions={0} | all-to-all | bytes 294912 | tf_op jit(solution)/shard_map/rows/all_to_all | solution.py:477
  42.0 0.2 mix.1
  42.2 12.6 %all_to_all.27.mixed_ref = bf16[16,64,128]{2,1,0:T(8,128)(2,1)S(1)} all-to-all(bf16[16,64,128]{2,1,0:T(8,128)(2,1)S(1)} %mix.1), channel_id=1, replica_groups=mesh['grp'=2,'ep'=16] {'ep'}, dimensions={0} | all-to-all | bytes 524288 | tf_op jit(solution)/shard_map/mixed/all_to_all | solution.py:487
  54.8 8.9 %expert.1 = (bf16[16,4,2048]{2,1,0:T(4,128)(2,1)S(1)}, f32[4,2048]{1,0:T(4,128)S(1)}) custom-call(bf16[16,64,128]{2,1,0:T(8,128)(2,1)S(1)} %all_to_all.27.mixed_ref, bf16[16,4,1152]{2,1,0:T(4,128)(2,1)S(1)} %all_to_all.26.rows_ref, f32[1,2048]{1,0:T(1,128)S(1)} %get-tuple-element.26.gain_ref, bf16[2048,1792]{1,0:T(8,128)(2,1)} %wg_hbm.1, ...), custom_call_target="tpu_custom_call" | custom-call | tf_op jit(solution)/shard_map/expert/pallas_call | solution.py:493
  63.7 12.7 %all_to_all.28.parts_ref = bf16[16,4,2048]{2,1,0:T(4,128)(2,1)S(1)} all-to-all(bf16[16,4,2048]{2,1,0:T(4,128)(2,1)S(1)} %get-tuple-element.27), channel_id=1, replica_groups=mesh['grp'=2,'ep'=16] {'ep'}, dimensions={0} | all-to-all | bytes 524288 | tf_op jit(solution)/shard_map/sums/all_to_all | solution.py:507
  76.4 0.7 finish.1
Async XLA Ops:
  0.6 13.9 %all-to-all-start = ((bf16[16,4,128]{2,1,0:T(4,128)(2,1)}), bf16[16,4,128]{2,1,0:T(4,128)(2,1)S(1)}, u32[]{:S(2)}, u32[]{:S(2)}) async-start(bf16[16,4,128]{2,1,0:T(4,128)(2,1)} %bitcast.9), calls=%async_computation | async-start | bytes 32768 | tf_op jit(solution)/shard_map/slices/all_to_all | solution.py:407

commit v3 on v2

--- a/solution.py
+++ b/solution.py
@@ -7,11 +7,11 @@
 from jax.experimental.pallas import tpu as pltpu
 from jax.sharding import PartitionSpec as P
 
+
 HEADS = 16
 KV_HEADS = 4
 HEAD_DIM = 64
 FF = 7168
-EXPERTS = 4
 EPSILON = 1e-06
 
 GROUP = HEADS // KV_HEADS
@@ -19,6 +19,8 @@
 QUERY_WIDTH = HEADS * HEAD_DIM
 ROW_WIDTH = QUERY_WIDTH + 128
 BLOCK = 256
+FIRST_HEAD = 1
+SECOND_HEAD = 1
 F32 = jnp.float32
 BF16 = jnp.bfloat16
 VMEM = pltpu.VMEM
@@ -27,10 +29,6 @@
 
 def vmem_spec():
     return pl.BlockSpec(memory_space=VMEM)
-
-
-def smem_spec():
-    return pl.BlockSpec(memory_space=pltpu.SMEM)
 
 
 def stage_kernel(
@@ -47,7 +45,6 @@
     wk_hbm,
     wv_hbm,
     w_out_hbm,
-    key_hbm,
     my_gain_ref,
     scale_ref,
     column_ref,
@@ -56,7 +53,6 @@
     ffn_gain_ref,
     w_in_ref,
     w_out_ref,
-    key_ref,
     lengths_scr,
     routes_scr,
     logits_scr,
@@ -84,7 +80,6 @@
         start += source.shape[1]
     large += [
         (w_out_hbm, w_out_ref),
-        (key_hbm, key_ref),
     ]
     copies = [
         pltpu.make_async_copy(source, target, sems.at[index])
@@ -95,8 +90,8 @@
     for copy in copies[: len(small)]:
         copy.wait()
 
-    me = lax.axis_index("ep")
-    my_gain_ref[...] = mix_gain_scr[pl.ds(me, 1), :]
+    chip = lax.axis_index("ep") // 2
+    my_gain_ref[...] = mix_gain_scr[pl.ds(2 * chip, 2), :]
     own = tokens_scr[...].astype(F32)
     token_scale = lax.rsqrt(jnp.mean(own * own, axis=-1, keepdims=True) + EPSILON)
     scale_ref[...] = jnp.broadcast_to(token_scale, scale_ref.shape)
@@ -132,31 +127,55 @@
         copy.wait()
 
 
-def project_kernel(rows_ref, gain_ref, w_ref, out_ref):
-    shards, tokens, width = rows_ref.shape
-    rows = rows_ref[...].astype(F32).reshape(shards * tokens, width)
-    scaled = (rows * gain_ref[...]).astype(BF16)
-    part = jnp.dot(scaled, w_ref[...], preferred_element_type=F32)
-    out_ref[...] = part.astype(BF16).reshape(out_ref.shape)
+def project_kernel(rows_ref, gain_ref, w_ref, wq_ref, wk_ref, wv_ref, after_ref, out_ref):
+    chips, tokens, width = rows_ref.shape
+    share = width // 2
+    rows = rows_ref[...].astype(F32).reshape(chips * tokens, width)
+    first = rows[:, :share] * gain_ref[0:1, :]
+    second = rows[:, share:] * gain_ref[1:2, :]
+    even = lax.axis_index("ep") % 2 == 0
+    own = jnp.where(even, first, second).astype(BF16)
+    other = jnp.where(even, second, first).astype(BF16)
+    start = 0
+    for other_ref in (wq_ref, wk_ref, wv_ref):
+        size = other_ref.shape[1]
+        span = slice(start, start + size)
+        part = jnp.dot(own, w_ref[:, span], preferred_element_type=F32)
+        part = part + jnp.dot(other, other_ref[...], preferred_element_type=F32)
+        out_ref[:, :, span] = part.astype(BF16).reshape(chips, tokens, size)
+        start += size
 
 
 def attend_kernel(
+    heads_of,
     parts_ref,
     scale_ref,
     column_ref,
     head_gain_ref,
     share_ref,
-    key_ref,
+    key_hbm,
     value_hbm,
-    row_ref,
-    new_key_ref,
-    new_value_ref,
-    heads_scr,
-    value_ref,
-    sem,
+    wd_hbm,
+    *rest,
 ):
-    fetch = pltpu.make_async_copy(value_hbm, value_ref, sem)
-    fetch.start()
+    if heads_of:
+        wg_hbm, wu_hbm, wg_ref, wu_ref = *rest[:2], *rest[6:8]
+        rest = *rest[2:6], *rest[8:]
+    row_ref, new_key_ref, new_value_ref, wd_ref, heads_scr, key_ref, value_ref, sems = rest
+    fetches = [
+        pltpu.make_async_copy(key_hbm, key_ref, sems.at[0]),
+        pltpu.make_async_copy(value_hbm, value_ref, sems.at[1]),
+    ]
+    pieces = [(wd_hbm, wd_ref)]
+    if heads_of:
+        pieces += [(wg_hbm.at[:, : wg_ref.shape[1]], wg_ref)]
+        pieces += [(wu_hbm.at[:, : wu_ref.shape[1]], wu_ref)]
+    later = [
+        pltpu.make_async_copy(source, target, sems.at[2 + index])
+        for index, (source, target) in enumerate(pieces)
+    ]
+    for fetch in fetches + later:
+        fetch.start()
     shards, tokens, _ = parts_ref.shape
     cache_len = key_ref.shape[1]
     columns = tokens * HEADS
@@ -203,6 +222,7 @@
         lax.broadcasted_iota(jnp.int32, (BLOCK, BLOCK), 1)
         >= lax.broadcasted_iota(jnp.int32, (BLOCK, BLOCK), 0)
     ).astype(F32).astype(BF16)
+    fetches[0].wait()
     carry = jnp.zeros((1, columns), F32)
     attended = [jnp.zeros((HEADS, KEY_WIDTH), F32) for _ in range(tokens)]
     for block in range(cache_len // BLOCK - 1, -1, -1):
@@ -228,7 +248,7 @@
         weight = jnp.where(alive, jnp.exp(score + inclusive), 0.0)
         weight = weight.T.astype(BF16)
         if block == cache_len // BLOCK - 1:
-            fetch.wait()
+            fetches[1].wait()
         for token in range(tokens):
             attended[token] = attended[token] + jnp.dot(
                 weight[token * HEADS : (token + 1) * HEADS, :],
@@ -252,27 +272,49 @@
 
     for shard in range(shards):
         row_ref[shard, :, QUERY_WIDTH:] = share_ref[...]
-
-
-def mix_kernel(rows_ref, tokens_ref, w_ref, mixed_ref):
-    shards, tokens, width = tokens_ref.shape
-    total = shards * tokens
-    mixed = tokens_ref[...].astype(F32).reshape(total, width)
-    rows = rows_ref[...].astype(F32).reshape(total, ROW_WIDTH).astype(BF16)
-    for member in range(GROUP):
-        pieces = []
-        for group in range(KV_HEADS):
-            head = group * GROUP + member
-            pieces.append(w_ref[head * HEAD_DIM : (head + 1) * HEAD_DIM, :])
-        weight = jnp.concatenate(pieces, axis=0)
-        mixed = mixed + jnp.dot(
-            rows[:, member * KEY_WIDTH : (member + 1) * KEY_WIDTH],
-            weight,
-            preferred_element_type=F32,
-        )
-    mixed = mixed.astype(BF16)
-    for shard in range(shards):
-        mixed_ref[shard] = mixed
+    for fetch in later:
+        fetch.wait()
+
+
+def mix_kernel(rows_ref, tokens_ref, own_ref, other_ref, mixed_ref, gate_ref):
+    chips, tokens, width = tokens_ref.shape
+    total, share = chips * tokens, width // 2
+    rows = rows_ref[...].astype(F32).reshape(total, ROW_WIDTH)
+    gate_ref[...] = rows[:, QUERY_WIDTH:].astype(BF16)
+    rows = rows[:, :QUERY_WIDTH].astype(BF16)
+    sides = []
+    for w_ref in (own_ref, other_ref):
+        side = jnp.zeros((total, share), F32)
+        for member in range(GROUP):
+            pieces = []
+            for group in range(KV_HEADS):
+                head = group * GROUP + member
+                pieces.append(w_ref[head * HEAD_DIM : (head + 1) * HEAD_DIM, :])
+            side = side + jnp.dot(
+                rows[:, member * KEY_WIDTH : (member + 1) * KEY_WIDTH],
+                jnp.concatenate(pieces, axis=0),
+                preferred_element_type=F32,
+            )
+        sides.append(side)
+    even = lax.axis_index("ep") % 2 == 0
+    tokens_in = tokens_ref[...].astype(F32).reshape(total, width)
+    first = (tokens_in[:, :share] + jnp.where(even, sides[0], sides[1])).astype(BF16)
+    second = (tokens_in[:, share:] + jnp.where(even, sides[1], sides[0])).astype(BF16)
+    for chip in range(chips):
+        mixed_ref[chip, :, :share] = first
+        mixed_ref[chip, :, share:] = second
+
+
+def fetch_kernel(start, after_hbm, gate_hbm, up_hbm, gate_ref, up_ref, sems):
+    span = slice(start, start + gate_ref.shape[1])
+    copies = [
+        pltpu.make_async_copy(gate_hbm.at[:, span], gate_ref, sems.at[0]),
+        pltpu.make_async_copy(up_hbm.at[:, span], up_ref, sems.at[1]),
+    ]
+    for copy in copies:
+        copy.start()
+    for copy in copies:
+        copy.wait()
 
 
 def chunk_of(size):
@@ -280,72 +322,86 @@
 
 
 def expert_kernel(
-    mixed_ref,
-    rows_ref,
+    ready,
+    own_mixed_ref,
+    other_mixed_ref,
+    own_gate_ref,
+    other_gate_ref,
     gain_ref,
-    wg_hbm,
-    wu_hbm,
-    wd_hbm,
-    out_ref,
-    own_ref,
-    wg_ref,
-    wu_ref,
     wd_ref,
-    sems,
+    *rest,
 ):
-    size = wg_ref.shape[1]
+    heads = rest[: 2 * ready]
+    wg_hbm, wu_hbm, own_ref, other_ref, mine_ref, wg_ref, wu_ref, sems = rest[2 * ready :]
+    size = wd_ref.shape[0]
     chunk = chunk_of(size)
     steps = size // chunk
-    copies = []
-    for step in range(steps):
-        span = slice(step * chunk, (step + 1) * chunk)
+    place_of = {}
+    start = 0
+    for index in range(ready):
+        for offset in range(0, heads[2 * index].shape[1], chunk):
+            place_of[start // chunk] = (heads[2 * index], heads[2 * index + 1], offset)
+            start += chunk
+    copies = {}
+    for step in range(start // chunk, steps):
+        offset = step * chunk - start
+        place_of[step] = (wg_ref, wu_ref, offset)
         for index, (source, target) in enumerate(((wg_hbm, wg_ref), (wu_hbm, wu_ref))):
-            copies.append(
-                pltpu.make_async_copy(
-                    source.at[:, span], target.at[:, span], sems.at[index, step]
-                )
+            copies[index, step] = pltpu.make_async_copy(
+                source.at[:, step * chunk : (step + 1) * chunk],
+                target.at[:, offset : offset + chunk],
+                sems.at[index, step],
             )
-    for step in range(steps):
-        span = slice(step * chunk, (step + 1) * chunk)
-        copies.append(
-            pltpu.make_async_copy(wd_hbm.at[span, :], wd_ref.at[span, :], sems.at[2, step])
-        )
-    for copy in copies:
+    for copy in copies.values():
         copy.start()
 
-    total, features = mixed_ref.shape[-2], gain_ref.shape[1]
-    shards, tokens = rows_ref.shape[:2]
-    if len(mixed_ref.shape) == 3:
-        mixed = jnp.concatenate([mixed_ref[s].astype(F32) for s in range(mixed_ref.shape[0])], axis=-1)
-    else:
-        mixed = mixed_ref[...].astype(F32)
+    half = own_gate_ref.shape[0]
+    tokens = mine_ref.shape[0]
+    sides = []
+    for mixed_ref in (own_mixed_ref, other_mixed_ref):
+        if len(mixed_ref.shape) == 3:
+            pieces = [mixed_ref[chip].astype(F32) for chip in range(mixed_ref.shape[0])]
+            sides.append(jnp.concatenate(pieces, axis=-1))
+        else:
+            sides.append(mixed_ref[...].astype(F32))
     me = lax.axis_index("ep")
-    picked = lax.broadcasted_iota(jnp.int32, (tokens, total), 1) - me * tokens
-    picked = picked == lax.broadcasted_iota(jnp.int32, (tokens, total), 0)
-    own_ref[...] = jnp.dot(
-        picked.astype(F32).astype(BF16), mixed.astype(BF16), preferred_element_type=F32
-    )
+    picked = lax.broadcasted_iota(jnp.int32, (tokens, half), 1) - me // 2 * tokens
+    picked = picked == lax.broadcasted_iota(jnp.int32, (tokens, half), 0)
+    mine_ref[...] = jnp.dot(
+        picked.astype(F32).astype(BF16), sides[0].astype(BF16), preferred_element_type=F32
+    )
+    mixed = jnp.concatenate(sides, axis=0)
     scale = lax.rsqrt(jnp.mean(mixed * mixed, axis=-1, keepdims=True) + EPSILON)
     expert_in = (mixed * scale * gain_ref[...]).astype(BF16)
-    gates = rows_ref[:, :, QUERY_WIDTH:].astype(F32).reshape(total, 128)
+    gates = jnp.concatenate(
+        [own_gate_ref[...].astype(F32), other_gate_ref[...].astype(F32)], axis=0
+    )
     lane = lax.broadcasted_iota(jnp.int32, gates.shape, 1)
     gate = jnp.where(lane % 64 == me // (FF // size), gates, 0.0)
     gate = jnp.sum(gate, axis=-1, keepdims=True)
-    hidden = []
-    for step in range(steps):
-        span = slice(step * chunk, (step + 1) * chunk)
-        copies[2 * step].wait()
-        value = jnp.dot(expert_in, wg_ref[:, span], preferred_element_type=F32)
-        copies[2 * step + 1].wait()
-        up = jnp.dot(expert_in, wu_ref[:, span], preferred_element_type=F32)
-        hidden.append((value / (1.0 + jnp.exp(-value)) * up * gate).astype(BF16))
     result = None
     for step in range(steps):
-        span = slice(step * chunk, (step + 1) * chunk)
-        copies[2 * steps + step].wait()
-        part = jnp.dot(hidden[step], wd_ref[span, :], preferred_element_type=F32)
+        gate_part, up_part, offset = place_of[step]
+        if (0, step) in copies:
+            copies[0, step].wait()
+            copies[1, step].wait()
+        value = jnp.dot(
+            expert_in, gate_part[:, offset : offset + chunk], preferred_element_type=F32
+        )
+        up = jnp.dot(
+            expert_in, up_part[:, offset : offset + chunk], preferred_element_type=F32
+        )
+        hidden = (value / (1.0 + jnp.exp(-value)) * up * gate).astype(BF16)
+        part = jnp.dot(
+            hidden, wd_ref[step * chunk : (step + 1) * chunk, :], preferred_element_type=F32
+        )
         result = part if result is None else result + part
-    out_ref[...] = result.astype(BF16).reshape(out_ref.shape)
+    own_ref[...] = result[:half].reshape(own_ref.shape)
+    other_ref[...] = result[half:].astype(BF16).reshape(other_ref.shape)
+
+
+def combine_kernel(own_ref, other_ref, out_ref):
+    out_ref[...] = (own_ref[...] + other_ref[...].astype(F32)).astype(BF16)
 
 
 def finish_kernel(parts_ref, mixed_ref, out_ref):
@@ -355,10 +411,9 @@
     out_ref[...] = total.astype(BF16)
 
 
-def call(kernel, name, outs, specs, scratch=(), limit=20):
+def call(kernel, outs, specs, scratch=(), limit=20):
     return pl.pallas_call(
         kernel,
-        name=name,
         out_shape=outs,
         in_specs=specs,
         out_specs=jax.tree.map(lambda _: vmem_spec(), outs),
@@ -396,15 +451,23 @@
     w_down,
 ):
     shards = lax.axis_size("ep")
+    chips = shards // 2
     token_rows, width = tokens.shape
     share = width // shards
-    all_rows = shards * token_rows
-    exchange = functools.partial(lax.all_to_all, axis_name="ep", split_axis=0, concat_axis=0)
+    half_rows = chips * token_rows
+    project_width = QUERY_WIDTH + 2 * KEY_WIDTH
     kept = pltpu.VMEM
-    project_width = QUERY_WIDTH + 2 * KEY_WIDTH
-
-    with jax.named_scope("slices"):
-        sliced = exchange(tokens.reshape(token_rows, shards, share).transpose(1, 0, 2))
+    groups = [[2 * chip + core for chip in range(chips)] for core in range(2)]
+    exchange = functools.partial(
+        lax.all_to_all, axis_name="ep", split_axis=0, concat_axis=0, axis_index_groups=groups
+    )
+    mate = functools.partial(
+        lax.ppermute, axis_name="ep", perm=[(index, index ^ 1) for index in range(shards)]
+    )
+
+    sliced = exchange(tokens.reshape(token_rows, chips, 2 * share).transpose(1, 0, 2))
+    other_in = [mate(w_query), mate(w_key), mate(w_value)]
+    other_out = mate(w_out)
     staged = [
         lengths,
         routes.T,
@@ -419,13 +482,11 @@
         w_key,
         w_value,
         w_out,
-        cache_key,
-    ]
-    my_gain, scale, column, head_gain, gates, ffn_row, w_in, w_mix, key = call(
+    ]
+    my_gain, scale, column, head_gain, gates, ffn_row, w_in, w_mix = call(
         stage_kernel,
-        "stage",
         (
-            kept((1, share), F32),
+            kept((2, share), F32),
             kept((token_rows, 128), F32),
             kept((2, token_rows * HEADS), F32),
             kept((2, KEY_WIDTH), F32),
@@ -433,7 +494,6 @@
             kept((1, width), F32),
             kept((share, project_width), BF16),
             kept(w_out.shape, BF16),
-            kept(cache_key.shape, BF16),
         ),
         [hbm_spec()] * len(staged),
         [
@@ -450,68 +510,107 @@
     )(*[in_hbm(array) for array in staged])
     parts = call(
         project_kernel,
-        "project",
-        kept((shards, token_rows, project_width), BF16),
-        [vmem_spec()] * 3,
+        kept((chips, token_rows, project_width), BF16),
+        [vmem_spec()] * 6 + [pl.BlockSpec(memory_space=pl.ANY)],
         limit=8,
-    )(sliced, my_gain, w_in)
-    with jax.named_scope("partial"):
-        parts = exchange(parts)
-
-    rows, new_key, new_value = call(
-        attend_kernel,
-        "attend",
+    )(sliced, my_gain, w_in, *other_in, other_out)
+    parts = exchange(parts)
+
+    size = w_gate.shape[1]
+    chunk = chunk_of(size)
+    first_head = min(FIRST_HEAD, size // chunk) * chunk
+    second_head = min(SECOND_HEAD * chunk, size - first_head)
+    early = [in_hbm(w_gate), in_hbm(w_up)] if first_head else []
+    rows, new_key, new_value, wd_all, *heads = call(
+        functools.partial(attend_kernel, bool(early)),
         (
-            kept((shards, token_rows, ROW_WIDTH), BF16),
+            kept((chips, token_rows, ROW_WIDTH), BF16),
             jax.ShapeDtypeStruct((token_rows, KEY_WIDTH), BF16),
             jax.ShapeDtypeStruct((token_rows, KEY_WIDTH), BF16),
-        ),
-        [vmem_spec()] * 6 + [hbm_spec()],
+            kept(w_down.shape, BF16),
+        )
+        + tuple(kept((width, first_head), BF16) for _ in early),
+        [vmem_spec()] * 5 + [hbm_spec()] * (3 + len(early)),
         [
             pltpu.VMEM((token_rows, GROUP, KEY_WIDTH), F32),
+            pltpu.VMEM(cache_key.shape, BF16),
             pltpu.VMEM(cache_value.shape, BF16),
-            pltpu.SemaphoreType.DMA,
+            pltpu.SemaphoreType.DMA((5,)),
         ],
-    )(parts, scale, column, head_gain, gates, key, in_hbm(cache_value))
-    with jax.named_scope("rows"):
-        rows = exchange(rows)
-
-    mixed = call(
+    )(
+        parts,
+        scale,
+        column,
+        head_gain,
+        gates,
+        in_hbm(cache_key),
+        in_hbm(cache_value),
+        in_hbm(w_down),
+        *early,
+    )
+    rows = exchange(rows)
+
+    mixed, own_gate = call(
         mix_kernel,
-        "mix",
-        kept((shards, all_rows, share), BF16),
-        [vmem_spec()] * 3,
+        (kept((chips, half_rows, 2 * share), BF16), kept((half_rows, 128), BF16)),
+        [vmem_spec()] * 4,
         limit=8,
-    )(rows, sliced, w_mix)
-    with jax.named_scope("mixed"):
-        mixed = exchange(mixed)
-
-    if share % 128:
-        expert_rows = mixed.transpose(1, 0, 2).reshape(all_rows, width)
+    )(rows, sliced, w_mix, other_out)
+    other_gate = mate(own_gate)
+    mixed = exchange(mixed)
+    other_mixed = mate(mixed)
+    if second_head:
+        heads += call(
+            functools.partial(fetch_kernel, first_head),
+            (kept((width, second_head), BF16), kept((width, second_head), BF16)),
+            [pl.BlockSpec(memory_space=pl.ANY)] + [hbm_spec()] * 2,
+            [pltpu.SemaphoreType.DMA((2,))],
+            limit=4,
+        )(mixed, in_hbm(w_gate), in_hbm(w_up))
+
+    if 2 * share % 128:
+        both = [side.transpose(1, 0, 2).reshape(half_rows, width) for side in (mixed, other_mixed)]
     else:
-        expert_rows = mixed
-    sums, own = call(
-        expert_kernel,
-        "expert",
-        (kept((shards, token_rows, width), BF16), kept((token_rows, width), F32)),
-        [vmem_spec()] * 3 + [hbm_spec()] * 3,
+        both = [mixed, other_mixed]
+    tail = max(size - first_head - second_head, chunk)
+    own, other, mine = call(
+        functools.partial(expert_kernel, len(heads) // 2),
+        (
+            kept((chips, token_rows, width), F32),
+            kept((chips, token_rows, width), BF16),
+            kept((token_rows, width), F32),
+        ),
+        [vmem_spec()] * (6 + len(heads)) + [hbm_spec()] * 2,
         [
-            pltpu.VMEM(w_gate.shape, BF16),
-            pltpu.VMEM(w_up.shape, BF16),
-            pltpu.VMEM(w_down.shape, BF16),
-            pltpu.SemaphoreType.DMA((3, w_gate.shape[1] // chunk_of(w_gate.shape[1]))),
+            pltpu.VMEM((width, tail), BF16),
+            pltpu.VMEM((width, tail), BF16),
+            pltpu.SemaphoreType.DMA((2, size // chunk)),
         ],
-        limit=40,
-    )(expert_rows, rows, ffn_row, in_hbm(w_gate), in_hbm(w_up), in_hbm(w_down))
-    with jax.named_scope("sums"):
-        sums = exchange(sums)
+        limit=28,
+    )(
+        *both,
+        own_gate,
+        other_gate,
+        ffn_row,
+        wd_all,
+        *heads,
+        in_hbm(w_gate),
+        in_hbm(w_up),
+    )
+    other = mate(other)
+    sums = call(
+        combine_kernel,
+        kept((chips, token_rows, width), BF16),
+        [vmem_spec()] * 2,
+        limit=8,
+    )(own, other)
+    sums = exchange(sums)
     output = call(
         finish_kernel,
-        "finish",
         jax.ShapeDtypeStruct((token_rows, width), BF16),
         [vmem_spec()] * 2,
         limit=8,
-    )(sums, own)
+    )(sums, mine)
     return output, new_key, new_value
 
 

time: 77.5 us -> 70.7 us (0.912)
  blocking collectives: 47.6 us -> 38.6 us
  waiting for transfers between devices: 4.45 us -> 6.63 us
  starting transfers between devices: 7.42 us -> 8.98 us
  Pallas kernels: 16.9 us -> 15.4 us
    all_to_all x1, blocking collectives: 12.6 us -> 9.74 us  [local(): mixed = exchange(mixed)]
    all_to_all x1, blocking collectives: 12.7 us -> 9.97 us  [local(): sums = exchange(sums)]
    all_to_all x1, blocking collectives: 11.6 us -> 9.51 us  [local(): parts = exchange(parts)]
    ppermute x0 -> x7, starting transfers between devices: none -> 1.73 us  [the longest x3 1.07 us: local(): other_in = [mate(w_query), mate(w_key), mate(w_value)]]
    pallas_call x6 -> x8, Pallas kernels: 16.9 us -> 15.4 us  [the longest x1 5.85 us: local(): call(functools.partial(expert_kernel, len(heads) // 2), (kept((chips, tok...]
    all_to_all x1, blocking collectives: 10.8 us -> 9.34 us  [local(): rows = exchange(rows)]
    ppermute x0 -> x7, waiting for transfers between devices: none -> 1.35 us  [the longest x1 1.33 us: local(): other = mate(other)]
    all_to_all x1, waiting for transfers between devices: 4.45 us -> 5.28 us  [local(): exchange(tokens.reshape(token_rows, chips, 2 * share).transpose(1, 0, 2))]
  transfers between devices with their start and end apart: 1 -> 8, of which waited for: 1 -> 2; matrix products, arithmetic and copies ran while one was open for 0% -> 0% of each run, Pallas kernels for 3% -> 4%
where the time goes in v3:
time: 70.7 us; the launch traced here: 70.3 us
  blocking collectives  38.6 us (55%)
  Pallas kernels  15.4 us (22%)
  starting transfers between devices  8.98 us (13%)
  waiting for transfers between devices  6.63 us (9%)
  between operations  0.73 us (1%)
    all_to_all x1, blocking collectives, local(): sums = exchange(sums)  9.97 us
    all_to_all x1, blocking collectives, local(): mixed = exchange(mixed)  9.74 us
    all_to_all x1, blocking collectives, local(): parts = exchange(parts)  9.51 us
    all_to_all x1, blocking collectives, local(): rows = exchange(rows)  9.34 us
    all_to_all x1, starting transfers between devices, local(): exchange(tokens.reshape(token_rows, chips, 2 * share).transpose(1, 0, 2))  7.25 us
    pallas_call x1, Pallas kernels, local(): call(functools.partial(expert_kernel, len(heads) // 2), (kept((chips, tok...  5.85 us
    pallas_call x1, Pallas kernels, local(): call(functools.partial(attend_kernel, bool(early)), (kept((chips, token_r...  5.58 us
    all_to_all x1, waiting for transfers between devices, local(): exchange(tokens.reshape(token_rows, chips, 2 * share).transpose(1, 0, 2))  5.28 us
  transfers between devices with their start and end apart: 8, of which 2 were waited for; matrix products, arithmetic and copies ran while one was open for 0% of the time, Pallas kernels for 4%

profile of v3, /device:TPU:0, one launch (start us, length us, event | category | flops | bytes accessed | tf_op | source)
XLA Modules:
  0.0 70.3 jit_solution(5836053685067567506)
XLA Ops:
  0.6 0.6 collective-permute-start
  1.2 0.1 collective-permute-start.3
  1.3 0.4 collective-permute-start.1
  1.7 0.1 collective-permute-start.2
  1.8 7.2 %all-to-all-start = ((bf16[8,4,256]{2,1,0:T(4,128)(2,1)}), bf16[8,4,256]{2,1,0:T(4,128)(2,1)S(1)}, u32[]{:S(2)}, u32[]{:S(2)}) async-start(bf16[8,4,256]{2,1,0:T(4,128)(2,1)} %bitcast.9), calls=%async_computation | async-start | bytes 32768 | tf_op jit(solution)/shard_map/all_to_all | solution.py:468
  9.0 1.3 %shard_map.193 = (f32[2,128]{1,0:T(2,128)S(1)}, f32[4,128]{1,0:T(4,128)S(1)}, f32[2,64]{1,0:T(2,128)S(1)}, f32[2,256]{1,0:T(2,128)S(1)}, bf16[4,128]{1,0:T(4,128...) custom-call(s32[4]{0:T(128)} %lengths_hbm.1, s32[2,4]{1,0:T(2,128)} %bitcast.12, ...), custom_call_target="tpu_custom_call" | custom-call | tf_op jit(solution)/shard_map/pallas_call | solution.py:486
  10.3 5.3 %all-to-all-done.rows_ref.tokens_ref = bf16[8,4,256]{2,1,0:T(4,128)(2,1)S(1)} async-done(((bf16[8,4,256]{2,1,0:T(4,128)(2,1)}), bf16[8,4,256]{2,1,0:T(4,128)(2,1)S(1)}, u32[]{:S(2)}, u32[]{:S(2)}) %all-to-all-start) | async-done | bytes 16416 | tf_op jit(solution)/shard_map/all_to_all | solution.py:468
  15.6 0.0 collective-permute-done.1.wk_ref
  15.6 0.0 collective-permute-done.2.wv_ref
  15.6 0.0 collective-permute-done.wq_ref
  15.6 0.0 collective-permute-done.3.after_ref.other_ref
  15.6 0.2 shard_map.194
  15.9 9.5 %all_to_all.25.parts_ref = bf16[8,4,1536]{2,1,0:T(4,128)(2,1)S(1)} all-to-all(bf16[8,4,1536]{2,1,0:T(4,128)(2,1)S(1)} %shard_map.194), channel_id=1, replica_groups={{0,2,4,6,8,10,12,14},{1,3,5,7,9,11,13,15},{16,18,20,22,24,26,28,30},{17..., dimensions={0} | all-to-all | bytes 196608 | tf_op jit(solution)/shard_map/all_to_all | solution.py:517
  25.4 5.6 %shard_map.195 = (bf16[8,4,1152]{2,1,0:T(4,128)(2,1)S(1)}, bf16[4,256]{1,0:T(4,128)(2,1)}, bf16[4,256]{1,0:T(4,128)(2,1)}, bf16[1792,2048]{1,0:T(8,128)(2,1)S(1)...) custom-call(bf16[8,4,1536]{2,1,0:T(4,128)(2,1)S(1)} %all_to_all.25.parts_ref, ...), custom_call_target="tpu_custom_call" | custom-call | tf_op jit(solution)/shard_map/pallas_call | solution.py:524
  31.0 9.3 %all_to_all.26.rows_ref = bf16[8,4,1152]{2,1,0:T(4,128)(2,1)S(1)} all-to-all(bf16[8,4,1152]{2,1,0:T(4,128)(2,1)S(1)} %get-tuple-element.30), channel_id=1, replica_groups={{0,2,4,6,8,10,12,14},{1,3,5,7,9,11,13,15},{16,18,20,22,24,26,28,30},{17..., dimensions={0} | all-to-all | bytes 147456 | tf_op jit(solution)/shard_map/all_to_all | solution.py:551
  40.3 0.2 shard_map.196
  40.5 9.7 %all_to_all.27.after_hbm.own_mixed_ref = bf16[8,32,256]{2,1,0:T(8,128)(2,1)S(1)} all-to-all(bf16[8,32,256]{2,1,0:T(8,128)(2,1)S(1)} %get-tuple-element.32), channel_id=1, replica_groups={{0,2,4,6,8,10,12,14},{1,3,5,7,9,11,13,15},{16,18,20,22,24,26,28,30},{17..., dimensions={0} | all-to-all | bytes 262144 | tf_op jit(solution)/shard_map/all_to_all | solution.py:560
  50.3 0.0 collective-permute-start.4
  50.3 0.5 collective-permute-start.5
  50.8 1.6 %shard_map.197 = (bf16[2048,256]{1,0:T(8,128)(2,1)S(1)}, bf16[2048,256]{1,0:T(8,128)(2,1)S(1)}) custom-call(bf16[8,32,256]{2,1,0:T(8,128)(2,1)S(1)} %all_to_all.27.after_hbm.own_mixed_ref, bf16[2048,1792]{1,0:T(8,128)(2,1)} %rest_4_.1, bf16[2048,1792]{1,0:T(8,128)(2,1)} %rest_5_.1), custom_call_target="tpu_custom_call" | custom-call | tf_op jit(solution)/shard_map/pallas_call | solution.py:563
  52.4 0.0 collective-permute-done.5.other_gate_ref
  52.4 0.0 collective-permute-done.4.other_mixed_ref
  52.4 5.9 %shard_map.198 = (f32[8,4,2048]{2,1,0:T(4,128)S(1)}, bf16[8,4,2048]{2,1,0:T(4,128)(2,1)S(1)}, f32[4,2048]{1,0:T(4,128)S(1)}) custom-call(bf16[8,32,256]{2,1,0:T(8,128)(2,1)S(1)} %all_to_all.27.after_hbm.own_mixed_ref, bf16[8,32,256]{2,1,0:T(8,128)(2,1)S(1)} %collective-permute-done.4.other_mixed_ref, bf16[32,128]{1,0:T(8,128)(2,1)S(1)} %get-tuple-element.33.own_gate_ref, ...), custom_call_target="tpu_custom_call" | custom-call | tf_op jit(solution)/shard_map/pallas_call | solution.py:576
  58.3 0.1 collective-permute-start.6
  58.3 1.3 %collective-permute-done.6.other_ref = bf16[8,4,2048]{2,1,0:T(4,128)(2,1)S(1)} collective-permute-done((bf16[8,4,2048]{2,1,0:T(4,128)(2,1)S(1)}, bf16[8,4,2048]{2,1,0:T(4,128)(2,1)S(1)}, u32[]{:S(2)}, u32[]{:S(2)}) %collective-permute-start.6) | collective-permute-done | bytes 131104 | tf_op jit(solution)/shard_map/ppermute | solution.py:600
  59.7 0.1 shard_map.199
  59.7 10.0 %all_to_all.28.parts_ref = bf16[8,4,2048]{2,1,0:T(4,128)(2,1)S(1)} all-to-all(bf16[8,4,2048]{2,1,0:T(4,128)(2,1)S(1)} %shard_map.199), channel_id=1, replica_groups={{0,2,4,6,8,10,12,14},{1,3,5,7,9,11,13,15},{16,18,20,22,24,26,28,30},{17..., dimensions={0} | all-to-all | bytes 262144 | tf_op jit(solution)/shard_map/all_to_all | solution.py:607
  69.7 0.6 shard_map.200
Async XLA Ops:
  0.6 15.0 %collective-permute-start = (bf16[128,1024]{1,0:T(8,128)(2,1)}, bf16[128,1024]{1,0:T(8,128)(2,1)S(1)}, u32[]{:S(2)}, u32[]{:S(2)}) collective-permute-start(bf16[128,1024]{1,0:T(8,128)(2,1)} %wq_hbm.1), channel_id=1, source_target_pairs={{0,1},{1,0},{2,3},{3,2},{4,5},{5,4},{6,7},{7,6},{8,9},{9,8},{10,11... | collective-permute-start | bytes 786440 | tf_op jit(solution)/shard_map/ppermute | solution.py:469
  1.2 14.4 %collective-permute-start.3 = (bf16[1024,128]{1,0:T(8,128)(2,1)}, bf16[1024,128]{1,0:T(8,128)(2,1)S(1)}, u32[]{:S(2)}, u32[]{:S(2)}) collective-permute-start(bf16[1024,128]{1,0:T(8,128)(2,1)} %w_out_hbm.1), channel_id=1, source_target_pairs={{0,1},{1,0},{2,3},{3,2},{4,5},{5,4},{6,7},{7,6},{8,9},{9,8},{10,11... | collective-permute-start | bytes 786440 | tf_op jit(solution)/shard_map/ppermute | solution.py:470
  1.3 14.3 %collective-permute-start.1 = (bf16[128,256]{1,0:T(8,128)(2,1)}, bf16[128,256]{1,0:T(8,128)(2,1)S(1)}, u32[]{:S(2)}, u32[]{:S(2)}) collective-permute-start(bf16[128,256]{1,0:T(8,128)(2,1)} %wk_hbm.1), channel_id=1, source_target_pairs={{0,1},{1,0},{2,3},{3,2},{4,5},{5,4},{6,7},{7,6},{8,9},{9,8},{10,11... | collective-permute-start | bytes 196616 | tf_op jit(solution)/shard_map/ppermute | solution.py:469
  1.7 13.9 %collective-permute-start.2 = (bf16[128,256]{1,0:T(8,128)(2,1)}, bf16[128,256]{1,0:T(8,128)(2,1)S(1)}, u32[]{:S(2)}, u32[]{:S(2)}) collective-permute-start(bf16[128,256]{1,0:T(8,128)(2,1)} %wv_hbm.1), channel_id=1, source_target_pairs={{0,1},{1,0},{2,3},{3,2},{4,5},{5,4},{6,7},{7,6},{8,9},{9,8},{10,11... | collective-permute-start | bytes 196616 | tf_op jit(solution)/shard_map/ppermute | solution.py:469
  1.8 13.8 %all-to-all-start = ((bf16[8,4,256]{2,1,0:T(4,128)(2,1)}), bf16[8,4,256]{2,1,0:T(4,128)(2,1)S(1)}, u32[]{:S(2)}, u32[]{:S(2)}) async-start(bf16[8,4,256]{2,1,0:T(4,128)(2,1)} %bitcast.9), calls=%async_computation | async-start | bytes 32768 | tf_op jit(solution)/shard_map/all_to_all | solution.py:468
  50.3 2.1 %collective-permute-start.4 = (bf16[8,32,256]{2,1,0:T(8,128)(2,1)S(1)}, bf16[8,32,256]{2,1,0:T(8,128)(2,1)S(1)}, u32[]{:S(2)}, u32[]{:S(2)}) collective-permute-start(bf16[8,32,256]{2,1,0:T(8,128)(2,1)S(1)} %all_to_all.27.after_hbm.own_mixed_ref), channel_id=1, source_target_pairs={{0,1},{1,0},{2,3},{3,2},{4,5},{5,4},{6,7},{7,6},{8,9},{9,8},{10,11... | collective-permute-start | bytes 393224 | tf_op jit(solution)/shard_map/ppermute | solution.py:561
  50.3 2.1 %collective-permute-start.5 = (bf16[32,128]{1,0:T(8,128)(2,1)S(1)}, bf16[32,128]{1,0:T(8,128)(2,1)S(1)}, u32[]{:S(2)}, u32[]{:S(2)}) collective-permute-start(bf16[32,128]{1,0:T(8,128)(2,1)S(1)} %get-tuple-element.33.own_gate_ref), channel_id=1, source_target_pairs={{0,1},{1,0},{2,3},{3,2},{4,5},{5,4},{6,7},{7,6},{8,9},{9,8},{10,11... | collective-permute-start | bytes 24584 | tf_op jit(solution)/shard_map/ppermute | solution.py:559
  58.3 1.4 %collective-permute-start.6 = (bf16[8,4,2048]{2,1,0:T(4,128)(2,1)S(1)}, bf16[8,4,2048]{2,1,0:T(4,128)(2,1)S(1)}, u32[]{:S(2)}, u32[]{:S(2)}) collective-permute-start(bf16[8,4,2048]{2,1,0:T(4,128)(2,1)S(1)} %get-tuple-element.41), channel_id=1, source_target_pairs={{0,1},{1,0},{2,3},{3,2},{4,5},{5,4},{6,7},{7,6},{8,9},{9,8},{10,11... | collective-permute-start | bytes 393224 | tf_op jit(solution)/shard_map/ppermute | solution.py:600
